TPU v7x, 128 devices: a whole 4x4x4 slice. The times are simulated.
128 devices in a mesh: kv: 16 (over z, x), tp: 8 (over y, core).
Axes of the slice: x: 4, y: 4, z: 4, core: 2. Of those that a mesh axis runs over, the one named last changes fastest.
Arguments:
- tokens: bfloat16 [32768, 2048], P('kv'), may hold values from -6 to 6
- norm_gain: bfloat16 [2048], replicated, may hold values from 0.099609375 to 1.8984375
- query_weight: bfloat16 [2048, 1024], P(None, 'tp'), may hold values from -0.125 to 0.125
- cmp_key_weight: bfloat16 [2048, 512], P(None, 'tp'), may hold values from -0.125 to 0.125
- cmp_value_weight: bfloat16 [2048, 512], P(None, 'tp'), may hold values from -0.125 to 0.125
- sel_key_weight: bfloat16 [2048, 512], P(None, 'tp'), may hold values from -0.125 to 0.125
- sel_value_weight: bfloat16 [2048, 512], P(None, 'tp'), may hold values from -0.125 to 0.125
- branch_weight: bfloat16 [2, 2048, 16], replicated, may hold values from -0.125 to 0.125
- key_embed: bfloat16 [8, 32, 64], P('tp'), may hold values from -3 to 3
- key_inner: bfloat16 [8, 2048, 64], P('tp'), may hold values from -0.125 to 0.125
- key_outer: bfloat16 [8, 64, 64], P('tp'), may hold values from -0.75 to 0.75
- value_embed: bfloat16 [8, 32, 64], P('tp'), may hold values from -3 to 3
- value_inner: bfloat16 [8, 2048, 64], P('tp'), may hold values from -0.125 to 0.125
- value_outer: bfloat16 [8, 64, 64], P('tp'), may hold values from -0.75 to 0.75
- out_weight: bfloat16 [1024, 2048], replicated, may hold values from -0.1875 to 0.1875
- chosen: int32 [8, 256, 8], P('tp'), may hold values from 0 to 511, as said below
Outputs:
- attended: bfloat16 [32768, 2048], P(('kv', 'tp'))
Inputs may be any that keep to these rules, and one draw needn't show every extreme that they name: `chosen`: each entry is the index of a block of 64 positions in the whole sequence. For every key head and query block, its 8 entries lie in 8 different aligned spans of 2048 positions (at most one from any span), and none lies inside the query block's own positions.
All inputs are finite; a program needn't handle non-finite values.
Results may differ from a plain program's by a relative error of at most 0.0075.
Values may be sent and summed in bfloat16 or wider, within the bound.
A program may use at most 128 MiB of HBM per device.

v0:
```python
import jax
import jax.numpy as jnp
from jax import lax
from jax.sharding import PartitionSpec as P

HEAD_DIM = 64
CMP_BLOCK = 32
SEL_BLOCK = 64
Q_BLOCK = 128
FAR_PICKS = 8


ROPE_BASE = 10000.0
norm_eps = 1e-06
masked_score = -1000000000.0


def copy_for_each(x, axis):
    peers = lax.axis_size(axis)
    return lax.all_to_all(jnp.broadcast_to(x[None], (peers, *x.shape)), axis, 0, 0, tiled=True)


def in_order(pieces, dim):
    shape = list(pieces.shape[1:])
    shape[dim] *= pieces.shape[0]
    return jnp.moveaxis(pieces, 0, dim).reshape(shape)


def collect(x, axis, dim):
    pieces = copy_for_each(x, axis)
    return in_order(pieces, dim)


def rotate(values_in, positions):
    half_dim = values_in.shape[-1] // 2
    inverse = ROPE_BASE ** (-jnp.arange(half_dim, dtype=jnp.float32) / half_dim)
    rotary_phases = positions.astype(jnp.float32)[:, None] * inverse[None, :]
    cosine = jnp.cos(rotary_phases)[:, None, :]
    sine = jnp.sin(rotary_phases)[:, None, :]
    first_half = values_in[..., :half_dim]
    second_half = values_in[..., half_dim:]
    return jnp.concatenate(
        [first_half * cosine - second_half * sine, second_half * cosine + first_half * sine],
        axis=-1,
    )


def summarize(raw_rows, embed, inner, outer):
    kv_local = embed.shape[0]
    block_count = raw_rows.shape[0] // CMP_BLOCK
    blocked = (
        raw_rows.reshape(block_count, CMP_BLOCK, kv_local, HEAD_DIM)
        .transpose(2, 0, 1, 3)
        .astype(jnp.float32)
    )
    blocked = (blocked + embed.astype(jnp.float32)[:, None]).astype(jnp.bfloat16)
    blocked = blocked.reshape(kv_local, block_count, CMP_BLOCK * HEAD_DIM)
    hidden = jax.nn.gelu(
        jnp.einsum("knc,kce->kne", blocked, inner, preferred_element_type=jnp.float32)
    ).astype(jnp.bfloat16)
    return jnp.einsum("kne,kef->knf", hidden, outer, preferred_element_type=jnp.float32).astype(
        jnp.bfloat16
    )


def per_device(
    tokens,
    norm_gain,
    query_weight,
    cmp_key_weight,
    cmp_value_weight,
    sel_key_weight,
    sel_value_weight,
    branch_weight,
    key_embed,
    key_inner,
    key_outer,
    value_embed,
    value_inner,
    value_outer,
    out_weight,
    chosen,
):
    tok_rows = tokens.shape[0]
    kv_local = key_embed.shape[0]
    heads_local = query_weight.shape[1] // HEAD_DIM
    group_size = heads_local // kv_local
    owners = lax.axis_size("kv")
    dev_index = lax.axis_index("kv")
    offset = dev_index * tok_rows
    positions = offset + jnp.arange(tok_rows, dtype=jnp.int32)
    scale = HEAD_DIM ** (-0.5)
    expanded_mask = tokens.astype(jnp.float32)
    normed = (
        expanded_mask
        * lax.rsqrt(jnp.mean(expanded_mask * expanded_mask, axis=-1, keepdims=True) + norm_eps)
        * norm_gain.astype(jnp.float32)
    ).astype(jnp.bfloat16)
    gate_cols = lax.dynamic_slice_in_dim(
        branch_weight, lax.axis_index("tp") * heads_local, heads_local, 2
    )
    q_width = heads_local * HEAD_DIM
    kv_width = kv_local * HEAD_DIM
    joined_weight = jnp.concatenate(
        [
            query_weight,
            cmp_key_weight,
            cmp_value_weight,
            sel_key_weight,
            sel_value_weight,
            gate_cols[0],
            gate_cols[1],
        ],
        axis=1,
    )
    projected = jnp.dot(normed, joined_weight, preferred_element_type=jnp.float32)
    bounds = [
        q_width,
        q_width + kv_width,
        q_width + 2 * kv_width,
        q_width + 3 * kv_width,
        q_width + 4 * kv_width,
        q_width + 4 * kv_width + heads_local,
    ]
    (
        query_part,
        cmp_key_part,
        cmp_value_part,
        sel_key_part,
        sel_value_part,
        gate_cmp_part,
        gate_sel_part,
    ) = jnp.split(projected, bounds, axis=1)
    query = query_part.reshape(tok_rows, heads_local, HEAD_DIM)
    q_plain = query.astype(jnp.bfloat16)
    q_turn = rotate(query, positions).astype(jnp.bfloat16)
    cmp_key = cmp_key_part.astype(jnp.bfloat16).reshape(tok_rows, kv_local, HEAD_DIM)
    cmp_value = cmp_value_part.astype(jnp.bfloat16).reshape(tok_rows, kv_local, HEAD_DIM)
    sel_key = rotate(sel_key_part.reshape(tok_rows, kv_local, HEAD_DIM), positions).astype(
        jnp.bfloat16
    )
    selected_value = sel_value_part.astype(jnp.bfloat16).reshape(tok_rows, kv_local, HEAD_DIM)
    gate_cmp = jax.nn.sigmoid(gate_cmp_part)
    gate_sel = jax.nn.sigmoid(gate_sel_part)
    summary = jnp.concatenate(
        [
            summarize(cmp_key, key_embed, key_inner, key_outer),
            summarize(cmp_value, value_embed, value_inner, value_outer),
        ],
        axis=-1,
    )
    summaries = collect(summary, "kv", 1)
    summary_count = summaries.shape[1]
    block_end = (jnp.arange(summary_count, dtype=jnp.int32) + 1) * CMP_BLOCK - 1
    q_group = q_plain.reshape(tok_rows, kv_local, group_size, HEAD_DIM).transpose(1, 0, 2, 3)
    cmp_scores = (
        jnp.einsum(
            "ktgd,kcd->ktgc", q_group, summaries[..., :HEAD_DIM], preferred_element_type=jnp.float32
        )
        * scale
    )
    usable = (block_end[None, :] <= positions[:, None])[None, :, None, :]
    cmp_probs = jax.nn.softmax(
        jnp.where(usable, cmp_scores, masked_score), axis=-1
    ) * usable.astype(jnp.float32)
    out_cmp = jnp.einsum(
        "ktgc,kcd->ktgd",
        cmp_probs.astype(jnp.bfloat16),
        summaries[..., HEAD_DIM:],
        preferred_element_type=jnp.float32,
    )
    out_cmp = out_cmp.transpose(1, 0, 2, 3).reshape(tok_rows, heads_local, HEAD_DIM)
    span_queries = tok_rows // Q_BLOCK
    span_blocks = tok_rows // SEL_BLOCK
    kv_sel = jnp.concatenate([sel_key, selected_value], axis=-1).transpose(1, 0, 2)
    all_picks = chosen.reshape(kv_local, owners, span_queries, FAR_PICKS)
    my_picks = lax.dynamic_index_in_dim(all_picks, dev_index, 1, keepdims=False)
    head_lane = jnp.arange(kv_local, dtype=jnp.int32)[:, None, None]
    matches = all_picks // span_blocks == dev_index
    wanted = jnp.sum(jnp.where(matches, all_picks % span_blocks, 0), axis=3)
    blocked = kv_sel.reshape(kv_local, span_blocks, SEL_BLOCK, 2 * HEAD_DIM)
    outgoing = blocked[head_lane, wanted]
    incoming = lax.all_to_all(outgoing, "kv", split_axis=1, concat_axis=1, tiled=True)
    source = my_picks // span_blocks
    query_lane = jnp.arange(span_queries, dtype=jnp.int32)[None, :, None]
    picked = incoming[head_lane, source, query_lane]
    own_keys = kv_sel.reshape(kv_local, span_queries, Q_BLOCK, 2 * HEAD_DIM)
    keys_all = jnp.concatenate(
        [own_keys, picked.reshape(kv_local, span_queries, FAR_PICKS * SEL_BLOCK, 2 * HEAD_DIM)],
        axis=2,
    )
    query_pos = positions.reshape(span_queries, Q_BLOCK)
    far_pos = (my_picks[..., None] * SEL_BLOCK + jnp.arange(SEL_BLOCK, dtype=jnp.int32)).reshape(
        kv_local, span_queries, FAR_PICKS * SEL_BLOCK
    )
    key_pos = jnp.concatenate([query_pos[None], far_pos], axis=2)
    q_sel = q_turn.reshape(span_queries, Q_BLOCK, kv_local, group_size, HEAD_DIM).transpose(
        2, 0, 1, 3, 4
    )
    sel_scores = (
        jnp.einsum(
            "knqgd,knmd->knqgm", q_sel, keys_all[..., :HEAD_DIM], preferred_element_type=jnp.float32
        )
        * scale
    )
    allowed_keys = key_pos[:, :, None, None, :] <= query_pos[None, :, :, None, None]
    sel_probs = jax.nn.softmax(jnp.where(allowed_keys, sel_scores, masked_score), axis=-1)
    out_sel = jnp.einsum(
        "knqgm,knmd->knqgd",
        sel_probs.astype(jnp.bfloat16),
        keys_all[..., HEAD_DIM:],
        preferred_element_type=jnp.float32,
    )
    out_sel = out_sel.transpose(1, 2, 0, 3, 4).reshape(tok_rows, heads_local, HEAD_DIM)
    mixed = (
        (gate_cmp[..., None] * out_cmp + gate_sel[..., None] * out_sel)
        .reshape(tok_rows, heads_local * HEAD_DIM)
        .astype(jnp.bfloat16)
    )
    head_rows = lax.all_to_all(mixed, "tp", split_axis=0, concat_axis=1, tiled=True)
    return jnp.dot(head_rows, out_weight, preferred_element_type=jnp.float32).astype(jnp.bfloat16)


def solution(mesh):
    placed = (
        P("kv", None),
        P(),
        P(None, "tp"),
        P(None, "tp"),
        P(None, "tp"),
        P(None, "tp"),
        P(None, "tp"),
        P(),
        P("tp", None, None),
        P("tp", None, None),
        P("tp", None, None),
        P("tp", None, None),
        P("tp", None, None),
        P("tp", None, None),
        P(),
        P("tp", None, None),
    )
    return jax.shard_map(
        per_device, mesh=mesh, in_specs=placed, out_specs=P(("kv", "tp"), None), check_vma=False
    )
```

profile of v0, /device:TPU:1, one launch (start us, length us, event | category | flops | bytes accessed | tf_op | source)
XLA Modules:
  0.0 171.9 jit_solution(5051237416359795915)
XLA Ops:
  0.0 0.8 convert_element_type.126
  0.8 5.1 %fusion.2 = f32[2048]{0:T(1024)S(1)} fusion(bf16[2048,2048]{1,0:T(8,128)(2,1)} %param.16), kind=kLoop, calls=%fused_computation.6 | loop fusion | flops 12580864 | bytes 8396800 | tf_op jit(solution)/shard_map/reduce_sum | solution.py:96
  6.0 0.8 dynamic-slice_bitcast_fusion
  7.4 1.0 copy.58
  8.4 1.0 copy.59
  9.5 1.0 copy.60
  10.5 1.0 copy.61
  12.4 5.5 %concatenate.68 = bf16[2048,388]{1,0:T(8,128)(2,1)} concatenate(bf16[2048,128]{1,0:T(8,128)(2,1)} %param.18, bf16[2048,64]{1,0:T(8,128)(2,1)} %copy.58, bf16[2048,64]{1,0:T(8,128)(2,1)} %copy.59, bf16[2048,64]{1,0:T(8,128)(2,1)} %copy.60, bf16[2048,64]{1,0:T(8,128)(2,1)} %copy.61, bf16[2048,2]{1,0:T(8,128)(2,1)S(1)} %copy.62, bf16[2048,2]{1,0:T(8,128)(2,1)S(1)} %copy.63), dimensions={1} | concatenate | bytes 3178496 | tf_op jit(solution)/shard_map/concatenate | solution.py:104
  17.8 9.4 %fusion.119 = (bf16[2048,388]{0,1:T(8,128)(2,1)S(1)}, f32[2048,388]{0,1:T(8,128)}) fusion(bf16[2048,388]{1,0:T(8,128)(2,1)} %concatenate.68, bf16[2048,2048]{1,0:T(8,128)(2,1)} %param.16, f32[2048]{0:T(1024)S(1)} %convert_element_type.126, f32[2048]{0:T(1024)S(1)} %add_rsqrt_fusion), kind=kOutput, calls=%fused_computation.179 | convolution fusion | flops 3272351744 | bytes 14761984 | tf_op jit(solution)/shard_map/dot_general | solution.py:116
  27.4 1.0 copy-done.11
  28.7 0.5 convert_element_type.132
  29.4 0.5 convert_element_type.138
  29.9 0.4 fusion.23
  30.3 0.4 fusion.24
  30.7 0.8 broadcast_in_dim.34
  31.5 8.5 %all-to-all-start = ((bf16[16,1,64,128]{3,2,1,0:T(8,128)(2,1)}), bf16[16,1,64,128]{3,2,1,0:T(8,128)(2,1)}, u32[]{:S(2)}, u32[]{:S(2)}) async-start(bf16[16,1,64,128]{3,2,1,0:T(8,128)(2,1)} %broadcast_in_dim.34), calls=%async_computation | async-start | bytes 524288 | tf_op jit(solution)/shard_map/all_to_all | solution.py:20
  40.2 1.7 %slice_bitcast_fusion.14 = (bf16[8,8,16,128]{3,1,2,0:T(8,128)(2,1)}, bf16[2048,64]{0,1:T(8,128)(2,1)S(1)}) fusion(bf16[2048,388]{0,1:T(8,128)(2,1)} %copy-done.11), kind=kLoop, calls=%fused_computation.176 | loop fusion | bytes 786432
  41.9 1.6 fusion.78
  43.5 1.1 slice_bitcast_fusion.4
  44.5 1.3 split.34
  46.7 1.8 %multiply_cosine_fusion.1 = (f32[2048,32]{0,1:T(8,128)}, f32[2048,32]{0,1:T(8,128)}) fusion(f32[32]{0:T(128)S(1)} %multiply_power_fusion, f32[2048]{0:T(1024)S(1)} %get-tuple-element.30), kind=kLoop, calls=%fused_computation.56 | loop fusion | flops 65536 | bytes 532608 | tf_op jit(solution)/shard_map/cos | solution.py:38
  48.5 1.1 fusion.35
  50.3 1.8 %broadcast_compare_fusion.1 = pred[16,128,640]{2,1,0:T(8,128)(4,1)} fusion(s32[16,128]{1,0:T(8,128)S(1)} %add_add_fusion, s32[16,640]{1,0:T(8,128)S(1)} %add_bitcast_fusion), kind=kLoop, calls=%fused_computation.30 | loop fusion | flops 1310720 | bytes 1359872 | tf_op jit(solution)/shard_map/le | solution.py:206
  52.0 0.5 pad_maximum_fusion.1
  52.5 3.1 %gather_fusion = bf16[256,64,128]{2,1,0:T(8,128)(2,1)} fusion(bf16[1,32,64,128]{3,2,1,0:T(8,128)(2,1)S(1)} %pad_maximum_fusion.1, s32[256]{0:T(256)S(1)} %reshape.731), kind=kCustom, calls=%fused_computation | custom fusion | bytes 8390656 | tf_op jit(solution)/shard_map/gather | solution.py:182
  55.8 6.8 %all-to-all-start.1 = ((bf16[1,16,16,64,128]{4,3,2,0,1:T(8,128)(2,1)}), bf16[1,16,16,64,128]{4,3,2,0,1:T(8,128)(2,1)}, u32[]{:S(2)}, u32[]{:S(2)}) async-start(bf16[1,16,16,64,128]{4,3,2,0,1:T(8,128)(2,1)} %bitcast.158), calls=%async_computation.1 | async-start | bytes 8388608 | tf_op jit(solution)/shard_map/all_to_all | solution.py:183
  62.6 2.1 %split.57 = bf16[2048,128]{0,1:T(8,128)(2,1)} slice(f32[2048,388]{0,1:T(8,128)} %get-tuple-element.24), slice={[0:2048], [0:128]} | slice | bytes 1048576 | tf_op jit(solution)/shard_map/split | solution.py:133
  64.9 0.8 copy.76
  65.7 0.8 copy.104
  66.5 0.7 copy.74
  67.2 0.8 copy.103
  68.5 4.2 %fusion.118 = (f32[2048,1024]{0,1:T(8,128)}, pred[2048,1024]{0,1:T(8,128)(4,1)S(1)}) fusion(s32[2048]{0:T(1024)S(1)} %get-tuple-element.29, s32[1024]{0:T(1024)S(1)} %multiply_add_fusion), kind=kLoop, calls=%fused_computation.178 | loop fusion | flops 4194304 | bytes 10498048 | tf_op jit(solution)/shard_map/convert_element_type | solution.py:165
  72.6 10.6 %fusion.121 = (f32[2048,2]{0,1:T(2,128)S(1)}, f32[2048,2,1024]{0,2,1:T(8,128)}) fusion(pred[2048,1024]{0,1:T(8,128)(4,1)S(1)} %get-tuple-element.20, bf16[2048,2,64]{0,2,1:T(8,128)(2,1)} %bitcast.173, bf16[1,1024,128]{2,1,0:T(8,128)(2,1)} %bitcast.14), kind=kOutput, calls=%fused_computation.181 | convolution fusion | flops 553649152 | bytes 19677184 | tf_op jit(solution)/shard_map/sub | solution.py:163
  83.3 9.4 %fusion.19 = f32[2048,2,64]{0,2,1:T(8,128)S(1)} fusion(f32[2048,2,1024]{0,2,1:T(8,128)} %get-tuple-element.28, f32[2048,1024]{0,1:T(8,128)} %get-tuple-element.19, f32[2048,2]{0,1:T(2,128)S(1)} %get-tuple-element.27, f32[2048,2]{0,1:T(2,128)S(1)} %copy-done.20, bf16[1,1024,128]{2,1,0:T(8,128)(2,1)} %bitcast.14), kind=kOutput, calls=%fused_computation.32 | convolution fusion | flops 549715968 | bytes 26509312 | tf_op jit(solution)/shard_map/ktgc,kcd->ktgd/dot_general | solution.py:166
  92.7 1.3 copy.96
  94.0 29.5 %all-to-all-done.1 = bf16[1,16,16,64,128]{4,3,2,0,1:T(8,128)(2,1)} async-done(((bf16[1,16,16,64,128]{4,3,2,0,1:T(8,128)(2,1)}), bf16[1,16,16,64,128]{4,3,2,0,1:T(8,128)(2,1)}, u32[]{:S(2)}, u32[]{:S(2)}) %all-to-all-start.1) | async-done | bytes 4194336 | tf_op jit(solution)/shard_map/all_to_all | solution.py:183
  123.5 4.5 %gather_fusion.1 = bf16[128,64,128]{2,1,0:T(8,128)(2,1)} fusion(bf16[1,16,16,64,128]{4,3,2,1,0:T(8,128)(2,1)} %bitcast.29, s32[128]{0:T(128)S(1)} %reshape.739), kind=kCustom, calls=%fused_computation.1 | custom fusion | bytes 4195840 | tf_op jit(solution)/shard_map/gather | solution.py:186
  127.9 2.9 %copy.83 = bf16[1,16,512,128]{2,3,1,0:T(8,128)(2,1)S(1)} copy(bf16[1,16,512,128]{3,2,1,0:T(8,128)(2,1)} %bitcast.159) | data formatting | bytes 4194304 | tf_op jit(solution)/shard_map/reshape | solution.py:189
  130.9 1.3 pad_maximum_fusion
  132.2 1.6 copy-done.2
  133.8 1.6 fusion.22
  135.4 7.2 %fusion.120 = (f32[16,128,2]{1,2,0:T(2,128)S(1)}, f32[16,128,2,640]{3,1,2,0:T(8,128)}) fusion(f32[16,128,2,640]{3,1,2,0:T(8,128)S(1)} %fusion.22, pred[16,128,640]{2,1,0:T(8,128)(4,1)S(1)} %copy-done.5), kind=kOutput, calls=%fused_computation.180 | output fusion | flops 15729279 | bytes 22298624 | tf_op jit(solution)/shard_map/sub | solution.py:207
  142.5 5.4 %fusion.18 = f32[16,128,2,64]{1,3,2,0:T(8,128)S(1)} fusion(f32[16,128,2,640]{3,1,2,0:T(8,128)} %get-tuple-element.26, f32[16,128,2]{1,2,0:T(2,128)S(1)} %get-tuple-element.25, bf16[1,16,640,128]{2,3,1,0:T(8,128)(2,1)S(1)} %copy-done.3), kind=kOutput, calls=%fused_computation.27 | convolution fusion | flops 340787200 | bytes 12861440 | tf_op jit(solution)/shard_map/knqgm,knmd->knqgd/dot_general | solution.py:208
  148.0 1.6 copy.84
  149.5 2.5 %reshape_transpose.10 = f32[8,256,128]{1,0,2:T(8,128)} reshape(f32[16,128,2,64]{1,0,3,2:T(8,128)} %copy.84) | data formatting | bytes 2097152 | tf_op jit(solution)/shard_map/reshape;transpose | solution.py:214
  152.1 1.6 fusion.26
  153.7 15.9 %all_to_all.26 = bf16[8,256,128]{1,2,0:T(8,128)(2,1)S(1)} all-to-all(bf16[8,256,128]{1,2,0:T(8,128)(2,1)S(1)} %copy.85), channel_id=1, replica_groups=mesh['kv'=16,'tp'=8] {'tp'}, dimensions={0} | all-to-all | bytes 1048576 | tf_op jit(solution)/shard_map/all_to_all | solution.py:220
  169.6 2.2 %convolution_convert_fusion = bf16[256,2048]{1,0:T(8,128)(2,1)} fusion(bf16[256,1024]{0,1:T(8,128)(2,1)S(1)} %bitcast.174, bf16[1024,2048]{1,0:T(8,128)(2,1)S(1)} %copy-done.23), kind=kOutput, calls=%fused_computation.31 | convolution fusion | flops 1074266112 | bytes 5767168 | tf_op jit(solution)/shard_map/dot_general | solution.py:221
  (98 shorter events, 4.9 us)
Async XLA Ops:
  0.0 29.9 %copy-start = (bf16[1,2048,64]{1,2,0:T(8,128)(2,1)S(1)}, bf16[1,2048,64]{1,2,0:T(8,128)(2,1)}, u32[]{:S(2)}) copy-start(bf16[1,2048,64]{1,2,0:T(8,128)(2,1)} %param.25) | copy-start | bytes 786436
  0.0 5.9 %copy-start.21 = (bf16[1,32,64]{2,1,0:T(8,128)(2,1)S(1)}, bf16[1,32,64]{2,1,0:T(8,128)(2,1)}, u32[]{:S(2)}) copy-start(bf16[1,32,64]{2,1,0:T(8,128)(2,1)} %param.24) | copy-start | bytes 12292
  0.0 6.0 %copy-start.22 = (bf16[1,32,64]{2,1,0:T(8,128)(2,1)S(1)}, bf16[1,32,64]{2,1,0:T(8,128)(2,1)}, u32[]{:S(2)}) copy-start(bf16[1,32,64]{2,1,0:T(8,128)(2,1)} %param.27) | copy-start | bytes 12292
  0.0 7.4 %copy-start.12 = (bf16[2048,64]{0,1:T(8,128)(2,1)S(1)}, bf16[2048,64]{0,1:T(8,128)(2,1)}, u32[]{:S(2)}) copy-start(bf16[2048,64]{0,1:T(8,128)(2,1)} %param.19) | copy-start | bytes 786436
  0.0 8.4 %copy-start.13 = (bf16[2048,64]{0,1:T(8,128)(2,1)S(1)}, bf16[2048,64]{0,1:T(8,128)(2,1)}, u32[]{:S(2)}) copy-start(bf16[2048,64]{0,1:T(8,128)(2,1)} %param.20) | copy-start | bytes 786436
  0.8 8.7 %copy-start.14 = (bf16[2048,64]{0,1:T(8,128)(2,1)S(1)}, bf16[2048,64]{0,1:T(8,128)(2,1)}, u32[]{:S(2)}) copy-start(bf16[2048,64]{0,1:T(8,128)(2,1)} %param.21) | copy-start | bytes 786436
  0.8 9.7 %copy-start.15 = (bf16[2048,64]{0,1:T(8,128)(2,1)S(1)}, bf16[2048,64]{0,1:T(8,128)(2,1)}, u32[]{:S(2)}) copy-start(bf16[2048,64]{0,1:T(8,128)(2,1)} %param.22) | copy-start | bytes 786436
  27.2 1.2 copy-start.11
  27.2 2.7 %copy-start.18 = (bf16[1,64,64]{2,1,0:T(8,128)(2,1)S(1)}, bf16[1,64,64]{2,1,0:T(8,128)(2,1)}, u32[]{:S(2)}) copy-start(bf16[1,64,64]{2,1,0:T(8,128)(2,1)} %param.26) | copy-start | bytes 24580
  27.2 3.0 %copy-start.16 = (bf16[1,2048,64]{1,2,0:T(8,128)(2,1)S(1)}, bf16[1,2048,64]{1,2,0:T(8,128)(2,1)}, u32[]{:S(2)}) copy-start(bf16[1,2048,64]{1,2,0:T(8,128)(2,1)} %param.28) | copy-start | bytes 786436
  27.2 3.1 %copy-start.19 = (bf16[1,64,64]{2,1,0:T(8,128)(2,1)S(1)}, bf16[1,64,64]{2,1,0:T(8,128)(2,1)}, u32[]{:S(2)}) copy-start(bf16[1,64,64]{2,1,0:T(8,128)(2,1)} %param.29) | copy-start | bytes 24580
  27.2 12.8 %copy-start.17 = (s32[1,256,8]{1,2,0:T(8,128)S(1)}, s32[1,256,8]{1,2,0:T(8,128)}, u32[]{:S(2)}) copy-start(s32[1,256,8]{1,2,0:T(8,128)} %param.31) | copy-start | bytes 24580
  31.5 24.3 %all-to-all-start = ((bf16[16,1,64,128]{3,2,1,0:T(8,128)(2,1)}), bf16[16,1,64,128]{3,2,1,0:T(8,128)(2,1)}, u32[]{:S(2)}, u32[]{:S(2)}) async-start(bf16[16,1,64,128]{3,2,1,0:T(8,128)(2,1)} %broadcast_in_dim.34), calls=%async_computation | async-start | bytes 524288 | tf_op jit(solution)/shard_map/all_to_all | solution.py:20
  52.5 3.1 %copy-start.9 = (f32[2048,32]{0,1:T(8,128)S(1)}, f32[2048,32]{0,1:T(8,128)}, u32[]{:S(2)}) copy-start(f32[2048,32]{0,1:T(8,128)} %get-tuple-element.21) | copy-start | bytes 786436
  52.5 3.1 %copy-start.10 = (f32[2048,32]{0,1:T(8,128)S(1)}, f32[2048,32]{0,1:T(8,128)}, u32[]{:S(2)}) copy-start(f32[2048,32]{0,1:T(8,128)} %get-tuple-element.22) | copy-start | bytes 786436
  55.8 9.1 %copy-start.6 = (bf16[8,8,16,128]{3,1,2,0:T(8,128)(2,1)S(1)}, bf16[8,8,16,128]{3,1,2,0:T(8,128)(2,1)}, u32[]{:S(2)}) copy-start(bf16[8,8,16,128]{3,1,2,0:T(8,128)(2,1)} %get-tuple-element.11) | copy-start | bytes 786436
  55.8 67.7 %all-to-all-start.1 = ((bf16[1,16,16,64,128]{4,3,2,0,1:T(8,128)(2,1)}), bf16[1,16,16,64,128]{4,3,2,0,1:T(8,128)(2,1)}, u32[]{:S(2)}, u32[]{:S(2)}) async-start(bf16[1,16,16,64,128]{4,3,2,0,1:T(8,128)(2,1)} %bitcast.158), calls=%async_computation.1 | async-start | bytes 8388608 | tf_op jit(solution)/shard_map/all_to_all | solution.py:183
  72.6 10.6 %copy-start.20 = (f32[2048,2]{0,1:T(2,128)S(1)}, f32[2048,2]{0,1:T(2,128)}, u32[]{:S(2)}) copy-start(f32[2048,2]{0,1:T(2,128)} %get-tuple-element.7) | copy-start | bytes 49156
  127.9 5.8 %copy-start.7 = (bf16[2,4,16,8,128]{4,3,1,0,2:T(8,128)(2,1)S(1)}, bf16[2,4,16,8,128]{4,3,1,0,2:T(8,128)(2,1)}, u32[]{:S(2)}) copy-start(bf16[2,4,16,8,128]{4,3,1,0,2:T(8,128)(2,1)} %copy.104) | copy-start | bytes 786436
  130.8 2.9 %copy-start.8 = (bf16[2,4,16,8,128]{4,3,1,0,2:T(8,128)(2,1)S(1)}, bf16[2,4,16,8,128]{4,3,1,0,2:T(8,128)(2,1)}, u32[]{:S(2)}) copy-start(bf16[2,4,16,8,128]{4,3,1,0,2:T(8,128)(2,1)} %copy.103) | copy-start | bytes 786436
  132.2 1.6 copy-start.2
  133.8 1.6 copy-start.5
  135.3 7.2 %copy-start.3 = (bf16[1,16,640,128]{2,3,1,0:T(8,128)(2,1)S(1)}, bf16[1,16,640,128]{2,3,1,0:T(8,128)(2,1)}, u32[]{:S(2)}) copy-start(bf16[1,16,640,128]{2,3,1,0:T(8,128)(2,1)} %copy-done.2) | copy-start | bytes 7864324
  142.5 9.5 %copy-start.4 = (f32[16,8,8,256]{3,2,1,0:T(8,128)S(1)}, f32[16,8,8,256]{3,2,1,0:T(8,128)}, u32[]{:S(2)}) copy-start(f32[16,8,8,256]{3,2,1,0:T(8,128)} %copy.96) | copy-start | bytes 3145732
  152.1 17.6 %copy-start.23 = (bf16[1024,2048]{1,0:T(8,128)(2,1)S(1)}, bf16[1024,2048]{1,0:T(8,128)(2,1)}, u32[]{:S(2)}) copy-start(bf16[1024,2048]{1,0:T(8,128)(2,1)} %param.30) | copy-start | bytes 12582916
  152.1 19.8 %copy-start.1 = (bf16[1,2048,64]{1,2,0:T(8,128)(2,1)S(1)}, bf16[1,2048,64]{1,2,0:T(8,128)(2,1)}, u32[]{:S(2)}) copy-start(bf16[1,2048,64]{1,2,0:T(8,128)(2,1)} %param.25) | copy-start | bytes 786436
where the time goes:
time: 173 us; the launch traced here: 172 us
  local copies, waits for them, and re-layouts  44 us (25%)
  matrix products  39.3 us (23%)
  waiting for transfers between devices  29.5 us (17%)
  other arithmetic  27.4 us (16%)
  blocking collectives  15.9 us (9%)
  starting transfers between devices  15.3 us (9%)
    all_to_all x1, waiting for transfers between devices, per_device(): lax.all_to_all(outgoing, 'kv', split_axis=1, concat_axis=1, tiled=True)  29.5 us
    all_to_all x1, blocking collectives, per_device(): lax.all_to_all(mixed, 'tp', split_axis=0, concat_axis=1, tiled=True)  15.9 us
    sub x1, matrix products, per_device(): jax.nn.softmax(jnp.where(usable, cmp_scores, masked_score), axis=-1)  10.6 us
    unnamed x58, local copies, waits for them, and re-layouts  10.2 us
    dot_general x1, matrix products, per_device(): jnp.einsum('ktgc,kcd->ktgd', cmp_probs.astype(jnp.bfloat16), summaries[.....  9.4 us
    dot_general x1, matrix products, per_device(): jnp.dot(normed, joined_weight, preferred_element_type=jnp.float32)  9.36 us
    all_to_all x1, starting transfers between devices, copy_for_each(): lax.all_to_all(jnp.broadcast_to(x[None], (peers, *x.shape)), axis, 0, 0,...  8.48 us
    sub x1, other arithmetic, per_device(): jax.nn.softmax(jnp.where(allowed_keys, sel_scores, masked_score), axis=-1)  7.17 us
  transfers between devices with their start and end apart: 2, of which 1 were waited for; matrix products, arithmetic and copies ran while one was open for 27% of the time, Pallas kernels for 0%

commit v1 on v0

v1 whole, which is shorter than its diff:
```python
import math

import jax
import jax.numpy as jnp
import numpy as np
from jax import lax
from jax.experimental import pallas as pl
from jax.experimental.pallas import tpu as pltpu
from jax.sharding import PartitionSpec as P

HEAD_DIM = 64
CMP_BLOCK = 32
SEL_BLOCK = 64
Q_BLOCK = 128
FAR_PICKS = 8
ROPE_BASE = 10000.0
NORM_EPS = 1e-06
MESH = pl.DeviceIdType.MESH
NT = (((1,), (1,)), ((), ()))
NEG = -1e30
ROWS = 512


def rope_tables(seq):
    half = HEAD_DIM // 2
    inverse = ROPE_BASE ** (-np.arange(half, dtype=np.float64) / half)
    lane = np.arange(128) % half
    low = np.arange(64, dtype=np.float64)[:, None] * inverse[lane][None, :]
    high = np.arange(seq // 64, dtype=np.float64)[:, None] * 64.0 * inverse[lane][None, :]
    return tuple(np.asarray(f(a), np.float32) for a in (low, high) for f in (np.cos, np.sin))


def gelu(x):
    return 0.5 * x * (1.0 + jnp.tanh(math.sqrt(2.0 / math.pi) * (x + 0.044715 * (x * x * x))))


def project_kernel(
    x_ref, gain_ref, qw_ref, ck_ref, cv_ref, sk_ref, sv_ref, bw_ref, ke_ref, ki_ref, ko_ref, ve_ref, vi_ref, vo_ref,
    cl_ref, sl_ref, ch_ref, sh_ref,
    qp_ref, qt_ref, kv_ref, gate_ref, sum_ref,
    w_ref, bi_ref, xk_ref, xv_ref,
):
    step = pl.program_id(0)
    me = lax.axis_index("kv")
    tp = lax.axis_index("tp")

    @pl.when(step == 0)
    def _():
        gain = gain_ref[...].astype(jnp.float32)
        w_ref[0:128, :] = (qw_ref[...].astype(jnp.float32).T * gain).astype(jnp.bfloat16)
        for at, ref in ((128, sk_ref), (192, sv_ref), (256, ck_ref), (320, cv_ref)):
            w_ref[at : at + 64, :] = (ref[...].astype(jnp.float32) * gain).astype(jnp.bfloat16)
        r = lax.broadcasted_iota(jnp.int32, (128, 32), 0)
        c = lax.broadcasted_iota(jnp.int32, (128, 32), 1)
        want = jnp.where(r < 2, tp * 2 + r, 16 + tp * 2 + (r - 2))
        pick = jnp.where((r < 4) & (c == want), 1.0, 0.0).astype(jnp.bfloat16)
        gates = jnp.dot(pick, bw_ref[...].reshape(32, -1), preferred_element_type=jnp.float32)
        w_ref[384:512, :] = (gates * gain).astype(jnp.bfloat16)

    x = x_ref[...]
    xf = x.astype(jnp.float32)
    scale = lax.rsqrt(jnp.sum(xf * xf, axis=1, keepdims=True) * (1.0 / x.shape[1]) + NORM_EPS)
    y = lax.dot_general(x, w_ref[...], NT, preferred_element_type=jnp.float32) * scale

    lane = lax.broadcasted_iota(jnp.int32, (1, 128), 1)
    front = lane < 64
    flip = lane % 64 < 32
    sign = jnp.where(flip, -1.0, 1.0)
    cos, sin = [], []
    low_c, low_s = cl_ref[...], sl_ref[...]
    for g in range(ROWS // 64):
        at = me * 32 + step * (ROWS // 64) + g
        hc, hs = ch_ref[pl.ds(at, 1), :], sh_ref[pl.ds(at, 1), :]
        cos.append(low_c * hc - low_s * hs)
        sin.append(low_c * (hs * sign) + low_s * (hc * sign))
    cos = jnp.concatenate(cos, axis=0)
    sin = jnp.concatenate(sin, axis=0)

    def turn(v, c, s):
        swapped = jnp.where(flip, pltpu.roll(v, 96, 1), pltpu.roll(v, 32, 1))
        return v * c + swapped * s

    def by_head(v):
        v = v * (HEAD_DIM**-0.5)
        first = jnp.where(front, v, 0.0)
        second = jnp.where(front, pltpu.roll(v, 64, 1), 0.0)
        return jnp.stack([first, second]).astype(jnp.bfloat16)

    q = y[:, 0:128]
    qp_ref[...] = by_head(q)
    qt_ref[...] = by_head(turn(q, cos, sin))
    kv_ref[...] = turn(y[:, 128:256], jnp.where(front, cos, 1.0), jnp.where(front, sin, 0.0)).astype(jnp.bfloat16)
    gate_ref[...] = 1.0 / (1.0 + jnp.exp(-y[:, 384:512]))
    embed = jnp.concatenate([ke_ref[0], ve_ref[0]], axis=1).astype(jnp.float32)
    embed = jnp.concatenate([embed] * (ROWS // CMP_BLOCK), axis=0)
    raw = y[:, 256:384].astype(jnp.bfloat16).astype(jnp.float32)
    bi_ref[pl.ds(pl.multiple_of(step * ROWS, ROWS), ROWS), :] = raw + embed

    @pl.when(step == pl.num_programs(0) - 1)
    def _():
        n = bi_ref.shape[0] // CMP_BLOCK
        for t in range(0, CMP_BLOCK, 2):
            a = bi_ref[pl.ds(t, n, stride=CMP_BLOCK), :]
            b = bi_ref[pl.ds(t + 1, n, stride=CMP_BLOCK), :]
            xk_ref[:, t * 64 : t * 64 + 128] = jnp.where(front, a, pltpu.roll(b, 64, 1)).astype(jnp.bfloat16)
            xv_ref[:, t * 64 : t * 64 + 128] = jnp.where(front, pltpu.roll(a, 64, 1), b).astype(jnp.bfloat16)
        out = []
        for x_in, inner, outer in ((xk_ref, ki_ref, ko_ref), (xv_ref, vi_ref, vo_ref)):
            hidden = lax.dot_general(x_in[...], inner[0], NT, preferred_element_type=jnp.float32)
            hidden = gelu(hidden).astype(jnp.bfloat16)
            out.append(jnp.dot(hidden, outer[0], preferred_element_type=jnp.float32))
        sum_ref[...] = jnp.concatenate(out, axis=1).astype(jnp.bfloat16)


def project(tokens, gain, qw, ck, cv, sk, sv, bw, ke, ki, ko, ve, vi, vo, seq):
    rows, width = tokens.shape
    tables = rope_tables(seq)
    steps = rows // ROWS

    def full(a):
        return pl.BlockSpec(a.shape, lambda i, n=a.ndim: (0,) * n, pipeline_mode=pl.Buffered(1))

    rest = (gain, qw, ck, cv, sk, sv, bw, ke, ki, ko, ve, vi, vo, *tables)
    bf, f32 = jnp.bfloat16, jnp.float32
    return pl.pallas_call(
        project_kernel,
        grid=(steps,),
        in_specs=[pl.BlockSpec((ROWS, width), lambda i: (i, 0))] + [full(a) for a in rest],
        out_specs=[
            pl.BlockSpec((2, ROWS, 128), lambda i: (0, i, 0)),
            pl.BlockSpec((2, ROWS, 128), lambda i: (0, i, 0)),
            pl.BlockSpec((ROWS, 128), lambda i: (i, 0)),
            pl.BlockSpec((ROWS, 128), lambda i: (i, 0)),
            pl.BlockSpec((rows // CMP_BLOCK, 128), lambda i: (0, 0)),
        ],
        out_shape=[
            jax.ShapeDtypeStruct((2, rows, 128), bf),
            jax.ShapeDtypeStruct((2, rows, 128), bf),
            jax.ShapeDtypeStruct((rows, 128), bf),
            jax.ShapeDtypeStruct((rows, 128), f32),
            jax.ShapeDtypeStruct((rows // CMP_BLOCK, 128), bf),
        ],
        scratch_shapes=[
            pltpu.VMEM((512, width), bf),
            pltpu.VMEM((rows, 128), f32),
            pltpu.VMEM((rows // CMP_BLOCK, CMP_BLOCK * 64), bf),
            pltpu.VMEM((rows // CMP_BLOCK, CMP_BLOCK * 64), bf),
        ],
        compiler_params=pltpu.CompilerParams(dimension_semantics=("arbitrary",), vmem_limit_bytes=26 << 20),
        name="project",
    )(tokens, *rest)


def rel(dz, dx):
    return (dz % 4) * 4 + dx % 4


def transfer_plan():
    plan = [("x+", rel(0, 0), 0, 2, rel(0, -1)), ("x-", rel(0, 0), 0, 2, rel(0, 1))]
    plan += [("z+", rel(0, 0), 2, 2, rel(-1, 0)), ("z-", rel(0, 0), 2, 2, rel(1, 0))]
    plan += [("z+", rel(0, 0), 0, 2, rel(-1, 0)), ("z-", rel(0, 0), 0, 2, rel(1, 0))]
    plan += [("x+", rel(0, 0), 2, 2, rel(0, -1)), ("x-", rel(0, 0), 2, 2, rel(0, 1))]
    plan += [("x+", rel(0, -1), 0, 1, rel(0, 2)), ("x-", rel(0, 1), 1, 1, rel(0, 2))]
    plan += [("z+", rel(-1, 0), 2, 1, rel(2, 0)), ("z-", rel(1, 0), 3, 1, rel(2, 0))]
    for d in (-1, 1):
        plan += [("z+", rel(0, d), 0, 2, rel(-1, d)), ("z-", rel(0, d), 0, 2, rel(1, d))]
        plan += [("x+", rel(d, 0), 2, 2, rel(d, -1)), ("x-", rel(d, 0), 2, 2, rel(d, 1))]
    plan += [("z+", rel(-1, 0), 0, 1, rel(2, 0)), ("z-", rel(1, 0), 1, 1, rel(2, 0))]
    plan += [("x+", rel(0, -1), 2, 1, rel(0, 2)), ("x-", rel(0, 1), 3, 1, rel(0, 2))]
    plan += [("z+", rel(0, 2), 0, 2, rel(-1, 2)), ("z-", rel(0, 2), 0, 2, rel(1, 2))]
    plan += [("x+", rel(2, 0), 2, 2, rel(2, -1)), ("x-", rel(2, 0), 2, 2, rel(2, 1))]
    for d in (-1, 1):
        plan += [("z+", rel(-1, d), 0, 1, rel(2, d)), ("z-", rel(1, d), 1, 1, rel(2, d))]
        plan += [("x+", rel(d, -1), 2, 1, rel(d, 2)), ("x-", rel(d, 1), 3, 1, rel(d, 2))]
    plan += [("z+", rel(-1, 2), 0, 1, rel(2, 2)), ("z-", rel(1, 2), 1, 1, rel(2, 2))]
    plan += [("x+", rel(2, -1), 2, 1, rel(2, 2)), ("x-", rel(2, 1), 3, 1, rel(2, 2))]
    return plan


PLAN = transfer_plan()


def attend_kernel(
    chosen_ref, kv_ref, qp_ref, qt_ref, gate_ref, sum_ref,
    out_ref,
    span_ref, sums_ref, mix_ref, send_ref, local_sem, span_send, span_recv, sum_send, sum_recv, tp_send, tp_recv,
):
    me = lax.axis_index("kv")
    tp = lax.axis_index("tp")
    mz, mx = me // 4, me % 4
    step_to = {
        "x+": (mz * 4 + (mx + 1) % 4, tp),
        "x-": (mz * 4 + (mx + 3) % 4, tp),
        "z+": (((mz + 1) % 4) * 4 + mx, tp),
        "z-": (((mz + 3) % 4) * 4 + mx, tp),
    }
    own = pltpu.make_async_copy(kv_ref, span_ref.at[0], local_sem)
    own.start()
    barrier = pltpu.get_barrier_semaphore()
    for k in range(1, 16):
        pl.semaphore_signal(barrier, inc=1, device_id=((me + k) % 16, tp), device_id_type=MESH)
    for k in range(1, 8):
        pl.semaphore_signal(barrier, inc=1, device_id=(me, (tp + k) % 8), device_id_type=MESH)
    pl.semaphore_wait(barrier, 22)

    def sum_copy(k):
        return pltpu.make_async_remote_copy(
            src_ref=sum_ref, dst_ref=sums_ref.at[me], send_sem=sum_send.at[k - 1], recv_sem=sum_recv.at[k - 1],
            device_id=((me + k) % 16, tp), device_id_type=MESH,
        )

    for k in range(1, 16):
        sum_copy(k).start()
    sums_ref[me] = sum_ref[...]

    def span_copy(i):
        way, source, first, n, target = PLAN[i]
        return pltpu.make_async_remote_copy(
            src_ref=span_ref.at[source, pl.ds(first * 8, n * 8)],
            dst_ref=span_ref.at[target, pl.ds(first * 8, n * 8)],
            send_sem=span_send.at[i], recv_sem=span_recv.at[i],
            device_id=step_to[way], device_id_type=MESH,
        )

    brings = {}
    for i, (_, _, first, n, target) in enumerate(PLAN):
        for quarter in range(first, first + n):
            brings[target, quarter] = i
    arrived = set()

    def start(i):
        _, source, first, n, _ = PLAN[i]
        if source:
            for quarter in range(first, first + n):
                need = brings[source, quarter]
                if need not in arrived:
                    span_copy(need).wait_recv()
                    arrived.add(need)
        span_copy(i).start()

    own.wait()
    for i in range(8):
        start(i)
    for k in range(1, 16):
        sum_copy(k).wait_recv()

    lane = lax.broadcasted_iota(jnp.int32, (1, 128), 1)
    front = lane < 64
    base = me * 2048

    def join(first, second):
        return jnp.where(front, pltpu.roll(first, 64, 1), second)

    @pl.loop(0, 8)
    def _(t):
        at = pl.multiple_of(t * 256, 256)
        rows = base + at + lax.broadcasted_iota(jnp.int32, (256, 1), 0)
        limit = (rows + 1) // CMP_BLOCK
        column = lax.broadcasted_iota(jnp.int32, (256, 1024), 1)
        sums = sums_ref[...].reshape(1024, 128)
        out = []
        for h in range(2):
            s = lax.dot_general(qp_ref[h, pl.ds(at, 256), :], sums, NT, preferred_element_type=jnp.float32)
            s = jnp.where(column < limit, s, NEG)
            top = jnp.maximum(jnp.max(s, axis=1, keepdims=True), -1e20)
            p = jnp.exp(s - top)
            total = jnp.maximum(jnp.sum(p, axis=1, keepdims=True), 0.5)
            o = jnp.dot(p.astype(jnp.bfloat16), sums, preferred_element_type=jnp.float32)
            out.append(o * (gate_ref[pl.ds(at, 256), h : h + 1] / total))
        mix_ref[pl.ds(at, 256), :] = join(*out)

    for i in range(8, len(PLAN)):
        start(i)
    for i in range(len(PLAN)):
        if i not in arrived:
            span_copy(i).wait_recv()

    triangle = lax.broadcasted_iota(jnp.int32, (128, 128), 1) <= lax.broadcasted_iota(jnp.int32, (128, 128), 0)
    ty, core = tp // 2, tp % 2

    def target_of(i):
        pair = i // 2
        dy = jnp.where(pair == 0, 2, jnp.where(pair == 1, 1, jnp.where(pair == 2, 3, 0)))
        flip = jnp.where(pair == 3, 1 - i % 2, i % 2)
        return ((ty + dy) % 4) * 2 + (core + flip) % 2

    def tp_copy(i, to):
        return pltpu.make_async_remote_copy(
            src_ref=send_ref.at[i], dst_ref=out_ref.at[:, pl.ds(pl.multiple_of(tp * 128, 128), 128)],
            send_sem=tp_send.at[i], recv_sem=tp_recv.at[i], device_id=(me, to), device_id_type=MESH,
        )

    @pl.loop(0, 8)
    def _(i):
        to = target_of(i)
        for half in range(2):
            j = to * 2 + half
            at = pl.multiple_of(j * 128, 128)
            parts, bias = [span_ref[0, 2 * j], span_ref[0, 2 * j + 1]], []
            for c in range(FAR_PICKS):
                block = chosen_ref[0, c, me * 16 + j]
                span, inside = block // 32, block % 32
                slot = ((span // 4 + 4 - mz) % 4) * 4 + (span % 4 + 4 - mx) % 4
                parts.append(span_ref[slot, inside])
                bias.append(jnp.where(block * 64 < base + at, 0.0, NEG))
            keys = jnp.concatenate(parts, axis=0)
            q = jnp.concatenate([qt_ref[0, pl.ds(at, 128), :], qt_ref[1, pl.ds(at, 128), :]], axis=0)
            s = lax.dot_general(q, keys, NT, preferred_element_type=jnp.float32)
            mine = jnp.where(jnp.concatenate([triangle, triangle], axis=0), s[:, :128], NEG)
            far = [
                s[:, 128 + 128 * c : 256 + 128 * c] + jnp.where(front, bias[2 * c], bias[2 * c + 1])
                for c in range(FAR_PICKS // 2)
            ]
            s = jnp.concatenate([mine, *far], axis=1)
            p = jnp.exp(s - jnp.max(s, axis=1, keepdims=True))
            total = jnp.sum(p, axis=1, keepdims=True)
            o = jnp.dot(p.astype(jnp.bfloat16), keys, preferred_element_type=jnp.float32)
            gates = gate_ref[pl.ds(at, 128), :]
            first = o[:128] * (gates[:, 2:3] / total[:128])
            second = o[128:] * (gates[:, 3:4] / total[128:])
            mixed = (mix_ref[pl.ds(at, 128), :] + join(first, second)).astype(jnp.bfloat16)
            send_ref[i, half * 128 : half * 128 + 128, :] = mixed

            @pl.when(i == 7)
            def _():
                out_ref[half * 128 : half * 128 + 128, pl.ds(pl.multiple_of(tp * 128, 128), 128)] = mixed

        @pl.when(i < 7)
        def _():
            tp_copy(i, to).start()

    for i in range(7):
        tp_copy(i, target_of(i)).wait_recv()
    for i in range(7):
        tp_copy(i, target_of(i)).wait_send()
    for k in range(1, 16):
        sum_copy(k).wait_send()
    for i in range(len(PLAN)):
        span_copy(i).wait_send()


def attend(chosen, kv, qp, qt, gates, summary):
    vmem = pl.BlockSpec(memory_space=pltpu.VMEM)
    return pl.pallas_call(
        attend_kernel,
        in_specs=[pl.BlockSpec(memory_space=pltpu.SMEM), pl.BlockSpec(memory_space=pl.ANY), vmem, vmem, vmem, vmem],
        out_specs=vmem,
        out_shape=jax.ShapeDtypeStruct((256, 1024), jnp.bfloat16),
        scratch_shapes=[
            pltpu.VMEM((16, 32, 64, 128), jnp.bfloat16),
            pltpu.VMEM((16, 64, 128), jnp.bfloat16),
            pltpu.VMEM((2048, 128), jnp.float32),
            pltpu.VMEM((8, 256, 128), jnp.bfloat16),
            pltpu.SemaphoreType.DMA,
            pltpu.SemaphoreType.DMA((len(PLAN),)),
            pltpu.SemaphoreType.DMA((len(PLAN),)),
            pltpu.SemaphoreType.DMA((15,)),
            pltpu.SemaphoreType.DMA((15,)),
            pltpu.SemaphoreType.DMA((7,)),
            pltpu.SemaphoreType.DMA((7,)),
        ],
        compiler_params=pltpu.CompilerParams(collective_id=0, has_side_effects=True, vmem_limit_bytes=30 << 20),
        name="attend",
    )(chosen, kv.reshape(32, 64, 128), qp, qt, gates, summary)


def per_device(
    tokens, norm_gain, query_weight, cmp_key_weight, cmp_value_weight, sel_key_weight, sel_value_weight,
    branch_weight, key_embed, key_inner, key_outer, value_embed, value_inner, value_outer, out_weight, chosen,
):
    seq = tokens.shape[0] * lax.axis_size("kv")
    qp, qt, kv, gates, summary = project(
        tokens, norm_gain.reshape(1, -1), query_weight,
        cmp_key_weight.T, cmp_value_weight.T, sel_key_weight.T, sel_value_weight.T,
        branch_weight.transpose(0, 2, 1),
        key_embed, key_inner.transpose(0, 2, 1), key_outer,
        value_embed, value_inner.transpose(0, 2, 1), value_outer, seq,
    )
    rows = attend(chosen.transpose(0, 2, 1), kv, qp, qt, gates, summary)
    return jnp.dot(rows, out_weight, preferred_element_type=jnp.float32).astype(jnp.bfloat16)


def solution(mesh):
    placed = (
        P("kv", None), P(), P(None, "tp"), P(None, "tp"), P(None, "tp"), P(None, "tp"), P(None, "tp"), P(),
        P("tp", None, None), P("tp", None, None), P("tp", None, None), P("tp", None, None), P("tp", None, None),
        P("tp", None, None), P(), P("tp", None, None),
    )
    return jax.shard_map(
        per_device, mesh=mesh, in_specs=placed, out_specs=P(("kv", "tp"), None), check_vma=False
    )
```

time: 173 us -> 101 us (0.58)
  Pallas kernels: 0 us -> 79.9 us
  matrix products: 39.3 us -> 2.23 us
  waiting for transfers between devices: 29.5 us -> 0 us
  other arithmetic: 27.4 us -> 0 us
  local copies, waits for them, and re-layouts: 44 us -> 18 us
  blocking collectives: 15.9 us -> 0 us
  starting transfers between devices: 15.3 us -> 0 us
    pallas_call x0 -> x2, Pallas kernels: none -> 79.9 us  [the longest x1 70.9 us: attend(): pl.pallas_call(attend_kernel, in_specs=[pl.BlockSpec(memory_space=pltpu.S...]
    all_to_all x2 -> x0, waiting for transfers between devices: 29.5 us -> none  [the longest x1 29.5 us: per_device(): lax.all_to_all(outgoing, 'kv', split_axis=1, concat_axis=1, tiled=True)]
    dot_general x7 -> x1, matrix products: 28.7 us -> 2.23 us  [per_device(): jnp.dot(rows, out_weight, preferred_element_type=jnp.float32)]
    all_to_all x1 -> x0, blocking collectives: 15.9 us -> none  [per_device(): lax.all_to_all(mixed, 'tp', split_axis=0, concat_axis=1, tiled=True)]
    all_to_all x2 -> x0, starting transfers between devices: 15.3 us -> none  [the longest x1 8.48 us: copy_for_each(): lax.all_to_all(jnp.broadcast_to(x[None], (peers, *x.shape)), axis, 0, 0,...]
    sub x1 -> x0, matrix products: 10.6 us -> none  [per_device(): jax.nn.softmax(jnp.where(usable, cmp_scores, masked_score), axis=-1)]
    concatenate x13 -> x0, local copies, waits for them, and re-layouts: 9.58 us -> none  [the longest x1 5.46 us: per_device(): jnp.concatenate([query_weight, cmp_key_weight, cmp_value_weight, sel_key_...]
    gather x2 -> x0, local copies, waits for them, and re-layouts: 7.53 us -> none  [the longest x1 4.46 us: per_device(): picked = incoming[head_lane, source, query_lane]]
  transfers between devices with their start and end apart: 2 -> 0, of which waited for: 1 -> 0; matrix products, arithmetic and copies ran while one was open for 27% -> 0% of each run, Pallas kernels for 0% -> 0%
where the time goes in v1:
time: 101 us; the launch traced here: 100 us
  Pallas kernels  79.9 us (79%)
  local copies, waits for them, and re-layouts  18 us (18%)
  matrix products  2.23 us (2%)
    pallas_call x1, Pallas kernels, attend(): pl.pallas_call(attend_kernel, in_specs=[pl.BlockSpec(memory_space=pltpu.S...  70.9 us
    unnamed x38, local copies, waits for them, and re-layouts  17.3 us
    pallas_call x1, Pallas kernels, project(): pl.pallas_call(project_kernel, grid=(steps,), in_specs=[pl.BlockSpec((ROW...  8.95 us
    dot_general x1, matrix products, per_device(): jnp.dot(rows, out_weight, preferred_element_type=jnp.float32)  2.23 us

profile of v1, /device:TPU:1, one launch (start us, length us, event | category | flops | bytes accessed | tf_op | source)
XLA Modules:
  0.0 100.1 jit_solution(17200881441855907406)
XLA Ops:
  0.0 0.7 reshape.6.gain_ref
  0.7 0.0 copy-start
  0.7 3.4 %copy-done = bf16[2048,2048]{1,0:T(8,128)(2,1)S(1)} copy-done((bf16[2048,2048]{1,0:T(8,128)(2,1)S(1)}, bf16[2048,2048]{1,0:T(8,128)(2,1)}, u32[]{:S(2)}) %copy-start) | copy-done | bytes 8388632
  4.1 0.0 copy-start.1
  4.1 1.0 %copy-done.1 = bf16[2048,128]{1,0:T(8,128)(2,1)S(1)} copy-done((bf16[2048,128]{1,0:T(8,128)(2,1)S(1)}, bf16[2048,128]{1,0:T(8,128)(2,1)}, u32[]{:S(2)}) %copy-start.1) | copy-done | bytes 524312
  5.1 0.0 copy-start.2
  5.1 0.9 copy-done.2
  6.1 0.0 copy-start.3
  6.1 0.9 copy-done.3
  7.0 0.0 copy-start.4
  7.0 0.9 copy-done.4
  8.0 0.0 copy-start.5
  8.0 0.9 copy-done.5
  8.9 0.0 copy-start.6
  8.9 0.9 copy-done.6
  9.9 0.0 copy-start.7
  9.9 0.9 copy-done.7
  10.8 0.0 copy-start.8
  10.8 0.9 copy-done.8
  11.8 0.0 copy-start.9
  11.8 0.9 copy-done.9
  12.7 0.0 copy-start.10
  12.7 0.9 copy-done.10
  13.6 0.0 copy-start.11
  13.6 0.8 copy-done.11
  14.4 0.0 copy-start.12
  14.4 0.8 copy-done.12
  15.1 0.0 copy-start.13
  15.1 0.7 copy-done.13
  15.9 0.0 copy-start.14
  15.9 0.7 copy-done.14
  16.6 0.0 copy-start.15
  16.6 0.7 copy-done.15
  17.3 0.0 copy-start.16
  17.3 0.7 copy-done.16
  18.0 0.0 copy-start.17
  18.0 8.9 %project.1 = (bf16[2,2048,128]{2,1,0:T(8,128)(2,1)S(1)}, bf16[2,2048,128]{2,1,0:T(8,128)(2,1)S(1)}, bf16[2048,128]{1,0:T(8,128)(2,1)S(1)}, f32[2048,128]{1,0:T(8,128)S(1)}, bf16[64,128]{1,0:T(8,128)(2,1)S(1)}) custom-call(bf16[2048,2048]{1,0:T(8,128)(2,1)S(1)} %copy-done, bf16[1,2048]{1,0:T(2,128)(2,1)S(1)} %reshape.6.gain_ref, ...), custom_call_target="tpu_custom_call" | custom-call | tf_op jit(solution)/shard_map/project/pallas_call | solution.py:125
  26.9 0.0 copy-start.18
  26.9 0.0 copy-done.17
  27.0 70.9 %attend.1 = bf16[256,1024]{1,0:T(8,128)(2,1)S(1)} custom-call(s32[1,8,256]{2,1,0:T(8,128)S(1)} %bitcast.19, bf16[32,64,128]{2,1,0:T(8,128)(2,1)S(1)} %bitcast.11, bf16[2,2048,128]{2,1,0:T(8,128)(2,1)S(1)} %get-tuple-element.11.qp_ref, bf16[2,2048,128]{2,1,0:T(8,128)(2,1)S(1)} %get-tuple-element.12.qt_ref, f32[2048,128]{1,0:T(8,128)S(1)} %get-tuple-element.13.gate_ref, ...), custom_call_target="tpu_custom_call" | custom-call | tf_op jit(solution)/shard_map/attend/pallas_call | solution.py:344
  97.9 0.0 copy-done.18
  97.9 2.2 %convolution_convert_fusion = bf16[256,2048]{1,0:T(8,128)(2,1)} fusion(bf16[256,1024]{1,0:T(8,128)(2,1)S(1)} %attend.1, bf16[1024,2048]{1,0:T(8,128)(2,1)S(1)} %copy-done.18), kind=kOutput, calls=%fused_computation | convolution fusion | flops 1074266112 | bytes 5767168 | tf_op jit(solution)/shard_map/dot_general | solution.py:380
Async XLA Ops:
  0.7 3.4 %copy-start = (bf16[2048,2048]{1,0:T(8,128)(2,1)S(1)}, bf16[2048,2048]{1,0:T(8,128)(2,1)}, u32[]{:S(2)}) copy-start(bf16[2048,2048]{1,0:T(8,128)(2,1)} %x_ref.1) | copy-start | bytes 25165828
  4.1 1.0 %copy-start.1 = (bf16[2048,128]{1,0:T(8,128)(2,1)S(1)}, bf16[2048,128]{1,0:T(8,128)(2,1)}, u32[]{:S(2)}) copy-start(bf16[2048,128]{1,0:T(8,128)(2,1)} %qw_ref.1) | copy-start | bytes 1572868
  5.1 0.9 copy-start.2
  6.1 0.9 copy-start.3
  7.0 0.9 copy-start.4
  8.0 0.9 copy-start.5
  8.9 0.9 copy-start.6
  9.9 0.9 copy-start.7
  10.8 0.9 copy-start.8
  11.8 0.9 copy-start.9
  12.7 0.9 copy-start.10
  13.6 0.8 copy-start.11
  14.4 0.8 copy-start.12
  15.1 0.7 copy-start.13
  15.9 0.7 copy-start.14
  16.6 0.7 copy-start.15
  17.3 0.7 copy-start.16
  18.0 9.0 %copy-start.17 = (s32[1,256,8]{1,2,0:T(8,128)S(1)}, s32[1,256,8]{1,2,0:T(8,128)}, u32[]{:S(2)}) copy-start(s32[1,256,8]{1,2,0:T(8,128)} %param.35) | copy-start | bytes 24580
  26.9 71.0 %copy-start.18 = (bf16[1024,2048]{1,0:T(8,128)(2,1)S(1)}, bf16[1024,2048]{1,0:T(8,128)(2,1)}, u32[]{:S(2)}) copy-start(bf16[1024,2048]{1,0:T(8,128)(2,1)} %param.34) | copy-start | bytes 12582916

commit v2 on v1

v2 whole, which is shorter than its diff:
```python
import math

import jax
import jax.numpy as jnp
import numpy as np
from jax import lax
from jax.experimental import pallas as pl
from jax.experimental.pallas import tpu as pltpu
from jax.sharding import PartitionSpec as P

HEAD_DIM = 64
CMP_BLOCK = 32
SEL_BLOCK = 64
Q_BLOCK = 128
FAR_PICKS = 8
ROPE_BASE = 10000.0
NORM_EPS = 1e-06
MESH = pl.DeviceIdType.MESH
NT = (((1,), (1,)), ((), ()))
NEG = -1e30
ROWS = 512


def rope_tables(seq):
    half = HEAD_DIM // 2
    inverse = ROPE_BASE ** (-np.arange(half, dtype=np.float64) / half)
    lane = np.arange(128) % half
    low = np.arange(64, dtype=np.float64)[:, None] * inverse[lane][None, :]
    high = np.arange(seq // 64, dtype=np.float64)[:, None] * 64.0 * inverse[lane][None, :]
    return tuple(np.asarray(f(a), np.float32) for a in (low, high) for f in (np.cos, np.sin))


def gelu(x):
    return 0.5 * x * (1.0 + jnp.tanh(math.sqrt(2.0 / math.pi) * (x + 0.044715 * (x * x * x))))


def rel(dz, dx):
    return (dz % 4) * 4 + dx % 4


def transfer_plan():
    plan = []
    for q in (0, 2):
        plan += [("x+", rel(0, 0), q, 2, rel(0, -1)), ("x-", rel(0, 0), q, 2, rel(0, 1))]
        plan += [("z+", rel(0, 0), q, 2, rel(-1, 0)), ("z-", rel(0, 0), q, 2, rel(1, 0))]
    plan += [("x+", rel(0, -1), 0, 1, rel(0, 2)), ("x-", rel(0, 1), 1, 1, rel(0, 2))]
    plan += [("z+", rel(-1, 0), 2, 1, rel(2, 0)), ("z-", rel(1, 0), 3, 1, rel(2, 0))]
    for d in (-1, 1):
        plan += [("z+", rel(0, d), 0, 2, rel(-1, d)), ("z-", rel(0, d), 0, 2, rel(1, d))]
        plan += [("x+", rel(d, 0), 2, 2, rel(d, -1)), ("x-", rel(d, 0), 2, 2, rel(d, 1))]
    plan += [("z+", rel(-1, 0), 0, 1, rel(2, 0)), ("z-", rel(1, 0), 1, 1, rel(2, 0))]
    plan += [("x+", rel(0, -1), 2, 1, rel(0, 2)), ("x-", rel(0, 1), 3, 1, rel(0, 2))]
    plan += [("z+", rel(0, 2), 0, 2, rel(-1, 2)), ("z-", rel(0, 2), 0, 2, rel(1, 2))]
    plan += [("x+", rel(2, 0), 2, 2, rel(2, -1)), ("x-", rel(2, 0), 2, 2, rel(2, 1))]
    for d in (-1, 1):
        plan += [("z+", rel(-1, d), 0, 1, rel(2, d)), ("z-", rel(1, d), 1, 1, rel(2, d))]
        plan += [("x+", rel(d, -1), 2, 1, rel(d, 2)), ("x-", rel(d, 1), 3, 1, rel(d, 2))]
    plan += [("z+", rel(-1, 2), 0, 1, rel(2, 2)), ("z-", rel(1, 2), 1, 1, rel(2, 2))]
    plan += [("x+", rel(2, -1), 2, 1, rel(2, 2)), ("x-", rel(2, 1), 3, 1, rel(2, 2))]
    return plan


PLAN = transfer_plan()


def layer_kernel(
    chosen_ref, x_hbm, gain_hbm, qw_hbm, ck_hbm, cv_hbm, sk_hbm, sv_hbm, bw_hbm,
    ke_hbm, ki_hbm, ko_hbm, ve_hbm, vi_hbm, vo_hbm, cl_hbm, sl_hbm, ch_hbm, sh_hbm,
    out_ref,
    x_ref, gain_ref, qw_ref, ck_ref, cv_ref, sk_ref, sv_ref, bw_ref,
    ke_ref, ki_ref, ko_ref, ve_ref, vi_ref, vo_ref, cl_ref, sl_ref, ch_ref, sh_ref,
    w_ref, scale_ref, bi_ref, xk_ref, xv_ref, qp_ref, qt_ref, gate_ref, sum_ref,
    span_ref, sums_ref, mix_ref, send_ref,
    in_sem, x_sem, span_send, span_recv, sum_send, sum_recv, tp_send, tp_recv,
):
    me = lax.axis_index("kv")
    tp = lax.axis_index("tp")
    mz, mx = me // 4, me % 4
    width = x_ref.shape[-1]
    steps = x_ref.shape[0]

    small = [
        (gain_hbm, gain_ref), (sk_hbm, sk_ref), (sv_hbm, sv_ref), (ck_hbm, ck_ref), (cv_hbm, cv_ref),
        (cl_hbm, cl_ref), (sl_hbm, sl_ref), (ch_hbm.at[pl.ds(me * 32, 32)], ch_ref),
        (sh_hbm.at[pl.ds(me * 32, 32)], sh_ref), (ke_hbm, ke_ref), (ve_hbm, ve_ref),
        (ki_hbm, ki_ref), (ko_hbm, ko_ref), (vi_hbm, vi_ref), (vo_hbm, vo_ref), (qw_hbm, qw_ref), (bw_hbm, bw_ref),
    ]
    small = [pltpu.make_async_copy(a, b, in_sem.at[i]) for i, (a, b) in enumerate(small)]
    rows_in = [pltpu.make_async_copy(x_hbm.at[pl.ds(i * ROWS, ROWS)], x_ref.at[i], x_sem.at[i]) for i in range(steps)]
    for copy in small[:9]:
        copy.start()
    for copy in rows_in:
        copy.start()
    for copy in small[9:]:
        copy.start()

    barrier = pltpu.get_barrier_semaphore()
    for k in range(1, 16):
        pl.semaphore_signal(barrier, inc=1, device_id=((me + k) % 16, tp), device_id_type=MESH)
    for k in range(1, 8):
        pl.semaphore_signal(barrier, inc=1, device_id=(me, (tp + k) % 8), device_id_type=MESH)

    lane = lax.broadcasted_iota(jnp.int32, (1, 128), 1)
    front = lane < 64
    flip = lane % 64 < 32
    sign = jnp.where(flip, -1.0, 1.0)

    def angles(step):
        cos, sin = [], []
        low_c, low_s = cl_ref[...], sl_ref[...]
        for g in range(ROWS // 64):
            hc = ch_ref[pl.ds(step * (ROWS // 64) + g, 1), :]
            hs = sh_ref[pl.ds(step * (ROWS // 64) + g, 1), :]
            cos.append(low_c * hc - low_s * hs)
            sin.append(low_c * (hs * sign) + low_s * (hc * sign))
        return jnp.concatenate(cos, axis=0), jnp.concatenate(sin, axis=0)

    def turn(v, c, s):
        swapped = jnp.where(flip, pltpu.roll(v, 96, 1), pltpu.roll(v, 32, 1))
        return v * c + swapped * s

    for copy in small[:9]:
        copy.wait()
    gain = gain_ref[...].astype(jnp.float32).reshape(1, width)
    for at, ref in ((0, sk_ref), (64, sv_ref), (128, ck_ref), (192, cv_ref)):
        w_ref[at : at + 64, :] = (ref[...].astype(jnp.float32) * gain).astype(jnp.bfloat16)
    for copy in small[9:11]:
        copy.wait()
    embed = jnp.concatenate([ke_ref[0], ve_ref[0]], axis=1).astype(jnp.float32)
    embed = jnp.concatenate([embed] * (ROWS // CMP_BLOCK), axis=0)
    for copy in rows_in:
        copy.wait()

    @pl.loop(0, steps)
    def _(step):
        x = x_ref[step]
        xf = x.astype(jnp.float32)
        scale = lax.rsqrt(jnp.sum(xf * xf, axis=1, keepdims=True) * (1.0 / width) + NORM_EPS)
        scale_ref[step] = scale
        y = lax.dot_general(x, w_ref[...], NT, preferred_element_type=jnp.float32) * scale
        cos, sin = angles(step)
        kv = turn(y[:, 0:128], jnp.where(front, cos, 1.0), jnp.where(front, sin, 0.0)).astype(jnp.bfloat16)
        span_ref[0, pl.ds(step * (ROWS // 64), ROWS // 64)] = kv.reshape(ROWS // 64, 64, 128)
        raw = y[:, 128:256].astype(jnp.bfloat16).astype(jnp.float32)
        bi_ref[pl.ds(pl.multiple_of(step * ROWS, ROWS), ROWS), :] = raw + embed

    pl.semaphore_wait(barrier, 22)

    step_to = {
        "x+": (mz * 4 + (mx + 1) % 4, tp),
        "x-": (mz * 4 + (mx + 3) % 4, tp),
        "z+": (((mz + 1) % 4) * 4 + mx, tp),
        "z-": (((mz + 3) % 4) * 4 + mx, tp),
    }

    def sum_copy(k):
        return pltpu.make_async_remote_copy(
            src_ref=sum_ref, dst_ref=sums_ref.at[me], send_sem=sum_send.at[k - 1], recv_sem=sum_recv.at[k - 1],
            device_id=((me + k) % 16, tp), device_id_type=MESH,
        )

    def span_copy(i):
        way, source, first, n, target = PLAN[i]
        return pltpu.make_async_remote_copy(
            src_ref=span_ref.at[source, pl.ds(first * 8, n * 8)],
            dst_ref=span_ref.at[target, pl.ds(first * 8, n * 8)],
            send_sem=span_send.at[i], recv_sem=span_recv.at[i],
            device_id=step_to[way], device_id_type=MESH,
        )

    brings = {}
    for i, (_, _, first, n, target) in enumerate(PLAN):
        for quarter in range(first, first + n):
            brings[target, quarter] = i
    arrived = set()

    def start(i):
        _, source, first, n, _ = PLAN[i]
        if source:
            for quarter in range(first, first + n):
                need = brings[source, quarter]
                if need not in arrived:
                    span_copy(need).wait_recv()
                    arrived.add(need)
        span_copy(i).start()

    for i in range(4):
        start(i)

    for copy in small[11:]:
        copy.wait()
    count = bi_ref.shape[0] // CMP_BLOCK
    for t in range(0, CMP_BLOCK, 2):
        a = bi_ref[pl.ds(t, count, stride=CMP_BLOCK), :]
        b = bi_ref[pl.ds(t + 1, count, stride=CMP_BLOCK), :]
        xk_ref[:, t * 64 : t * 64 + 128] = jnp.where(front, a, pltpu.roll(b, 64, 1)).astype(jnp.bfloat16)
        xv_ref[:, t * 64 : t * 64 + 128] = jnp.where(front, pltpu.roll(a, 64, 1), b).astype(jnp.bfloat16)
    summary = []
    for x_in, inner, outer in ((xk_ref, ki_ref, ko_ref), (xv_ref, vi_ref, vo_ref)):
        hidden = lax.dot_general(x_in[...], inner[0], NT, preferred_element_type=jnp.float32)
        hidden = gelu(hidden).astype(jnp.bfloat16)
        summary.append(jnp.dot(hidden, outer[0], preferred_element_type=jnp.float32))
    summary = jnp.concatenate(summary, axis=1).astype(jnp.bfloat16)
    sum_ref[...] = summary
    sums_ref[me] = summary
    for i in range(4, 8):
        start(i)

    w_ref[0:128, :] = (qw_ref[...].astype(jnp.float32).T * gain).astype(jnp.bfloat16)
    r = lax.broadcasted_iota(jnp.int32, (128, 32), 0)
    c = lax.broadcasted_iota(jnp.int32, (128, 32), 1)
    want = jnp.where(r < 2, tp * 2 + r, 16 + tp * 2 + (r - 2))
    pick = jnp.where((r < 4) & (c == want), 1.0, 0.0).astype(jnp.bfloat16)
    gates = jnp.dot(pick, bw_ref[...].reshape(32, width), preferred_element_type=jnp.float32)
    w_ref[128:256, :] = (gates * gain).astype(jnp.bfloat16)
    for k in range(1, 16):
        sum_copy(k).start()

    def by_head(v):
        v = v * (HEAD_DIM**-0.5)
        first = jnp.where(front, v, 0.0)
        second = jnp.where(front, pltpu.roll(v, 64, 1), 0.0)
        return jnp.stack([first, second]).astype(jnp.bfloat16)

    @pl.loop(0, steps)
    def _(step):
        y = lax.dot_general(x_ref[step], w_ref[...], NT, preferred_element_type=jnp.float32) * scale_ref[step]
        at = pl.ds(pl.multiple_of(step * ROWS, ROWS), ROWS)
        q = y[:, 0:128]
        qp_ref[:, at, :] = by_head(q)
        qt_ref[:, at, :] = by_head(turn(q, *angles(step)))
        gate_ref[at, :] = 1.0 / (1.0 + jnp.exp(-y[:, 128:256]))

    for i in range(8, 20):
        start(i)
    for k in range(1, 16):
        sum_copy(k).wait_recv()

    base = me * 2048

    def join(first, second):
        return jnp.where(front, pltpu.roll(first, 64, 1), second)

    @pl.loop(0, 8)
    def _(t):
        at = pl.multiple_of(t * 256, 256)
        rows = base + at + lax.broadcasted_iota(jnp.int32, (256, 1), 0)
        limit = (rows + 1) // CMP_BLOCK
        column = lax.broadcasted_iota(jnp.int32, (256, 1024), 1)
        sums = sums_ref[...].reshape(1024, 128)
        out = []
        for h in range(2):
            s = lax.dot_general(qp_ref[h, pl.ds(at, 256), :], sums, NT, preferred_element_type=jnp.float32)
            s = jnp.where(column < limit, s, NEG)
            top = jnp.maximum(jnp.max(s, axis=1, keepdims=True), -1e20)
            p = jnp.exp(s - top)
            total = jnp.maximum(jnp.sum(p, axis=1, keepdims=True), 0.5)
            o = jnp.dot(p.astype(jnp.bfloat16), sums, preferred_element_type=jnp.float32)
            out.append(o * (gate_ref[pl.ds(at, 256), h : h + 1] / total))
        mix_ref[pl.ds(at, 256), :] = join(*out)

    for i in range(20, len(PLAN)):
        start(i)

    for i in range(len(PLAN)):
        if i not in arrived:
            span_copy(i).wait_recv()

    triangle = lax.broadcasted_iota(jnp.int32, (128, 128), 1) <= lax.broadcasted_iota(jnp.int32, (128, 128), 0)
    ty, core = tp // 2, tp % 2

    def target_of(i):
        pair = i // 2
        dy = jnp.where(pair == 0, 2, jnp.where(pair == 1, 1, jnp.where(pair == 2, 3, 0)))
        flip = jnp.where(pair == 3, 1 - i % 2, i % 2)
        return ((ty + dy) % 4) * 2 + (core + flip) % 2

    def tp_copy(i, to):
        return pltpu.make_async_remote_copy(
            src_ref=send_ref.at[i], dst_ref=out_ref.at[:, pl.ds(pl.multiple_of(tp * 128, 128), 128)],
            send_sem=tp_send.at[i], recv_sem=tp_recv.at[i], device_id=(me, to), device_id_type=MESH,
        )

    @pl.loop(0, 8)
    def _(i):
        to = target_of(i)
        for half in range(2):
            j = to * 2 + half
            at = pl.multiple_of(j * 128, 128)
            parts, bias = [span_ref[0, 2 * j], span_ref[0, 2 * j + 1]], []
            for c in range(FAR_PICKS):
                block = chosen_ref[0, c, me * 16 + j]
                span, inside = block // 32, block % 32
                slot = ((span // 4 + 4 - mz) % 4) * 4 + (span % 4 + 4 - mx) % 4
                parts.append(span_ref[slot, inside])
                bias.append(jnp.where(block * 64 < base + at, 0.0, NEG))
            keys = jnp.concatenate(parts, axis=0)
            q = jnp.concatenate([qt_ref[0, pl.ds(at, 128), :], qt_ref[1, pl.ds(at, 128), :]], axis=0)
            s = lax.dot_general(q, keys, NT, preferred_element_type=jnp.float32)
            mine = jnp.where(jnp.concatenate([triangle, triangle], axis=0), s[:, :128], NEG)
            far = [
                s[:, 128 + 128 * c : 256 + 128 * c] + jnp.where(front, bias[2 * c], bias[2 * c + 1])
                for c in range(FAR_PICKS // 2)
            ]
            s = jnp.concatenate([mine, *far], axis=1)
            p = jnp.exp(s - jnp.max(s, axis=1, keepdims=True))
            total = jnp.sum(p, axis=1, keepdims=True)
            o = jnp.dot(p.astype(jnp.bfloat16), keys, preferred_element_type=jnp.float32)
            gates = gate_ref[pl.ds(at, 128), :]
            first = o[:128] * (gates[:, 2:3] / total[:128])
            second = o[128:] * (gates[:, 3:4] / total[128:])
            mixed = (mix_ref[pl.ds(at, 128), :] + join(first, second)).astype(jnp.bfloat16)
            send_ref[i, half * 128 : half * 128 + 128, :] = mixed

            @pl.when(i == 7)
            def _():
                out_ref[half * 128 : half * 128 + 128, pl.ds(pl.multiple_of(tp * 128, 128), 128)] = mixed

        @pl.when(i < 7)
        def _():
            tp_copy(i, to).start()

    for i in range(7):
        tp_copy(i, target_of(i)).wait_recv()
    for i in range(7):
        tp_copy(i, target_of(i)).wait_send()
    for k in range(1, 16):
        sum_copy(k).wait_send()
    for i in range(len(PLAN)):
        span_copy(i).wait_send()


def layer(chosen, tokens, rest, seq):
    rows, width = tokens.shape
    args = (tokens, *rest, *rope_tables(seq))
    bf, f32 = jnp.bfloat16, jnp.float32
    spans = seq // rows
    held = [pltpu.VMEM((rows // ROWS, ROWS, width), bf)]
    held += [pltpu.VMEM(a.shape, a.dtype) for a in args[1:-2]]
    held += [pltpu.VMEM((rows // 64, 128), f32)] * 2
    dma = pltpu.SemaphoreType.DMA
    return pl.pallas_call(
        layer_kernel,
        in_specs=[pl.BlockSpec(memory_space=pltpu.SMEM)] + [pl.BlockSpec(memory_space=pltpu.HBM)] * len(args),
        out_specs=pl.BlockSpec(memory_space=pltpu.VMEM),
        out_shape=jax.ShapeDtypeStruct((rows // 8, 1024), bf),
        scratch_shapes=held + [
            pltpu.VMEM((256, width), bf),
            pltpu.VMEM((rows // ROWS, ROWS, 1), f32),
            pltpu.VMEM((rows, 128), f32),
            pltpu.VMEM((rows // CMP_BLOCK, CMP_BLOCK * 64), bf),
            pltpu.VMEM((rows // CMP_BLOCK, CMP_BLOCK * 64), bf),
            pltpu.VMEM((2, rows, 128), bf),
            pltpu.VMEM((2, rows, 128), bf),
            pltpu.VMEM((rows, 128), f32),
            pltpu.VMEM((rows // CMP_BLOCK, 128), bf),
            pltpu.VMEM((spans, rows // 64, 64, 128), bf),
            pltpu.VMEM((spans, rows // CMP_BLOCK, 128), bf),
            pltpu.VMEM((rows, 128), f32),
            pltpu.VMEM((8, rows // 8, 128), bf),
            dma((17,)), dma((rows // ROWS,)), dma((len(PLAN),)), dma((len(PLAN),)),
            dma((15,)), dma((15,)), dma((7,)), dma((7,)),
        ],
        compiler_params=pltpu.CompilerParams(collective_id=0, has_side_effects=True, vmem_limit_bytes=67043328),
        name="layer",
    )(chosen, *args)


def per_device(
    tokens, norm_gain, query_weight, cmp_key_weight, cmp_value_weight, sel_key_weight, sel_value_weight,
    branch_weight, key_embed, key_inner, key_outer, value_embed, value_inner, value_outer, out_weight, chosen,
):
    seq = tokens.shape[0] * lax.axis_size("kv")
    rest = (
        norm_gain, query_weight,
        cmp_key_weight.T, cmp_value_weight.T, sel_key_weight.T, sel_value_weight.T,
        branch_weight.transpose(0, 2, 1),
        key_embed, key_inner.transpose(0, 2, 1), key_outer,
        value_embed, value_inner.transpose(0, 2, 1), value_outer,
    )
    rows = layer(chosen.transpose(0, 2, 1), tokens, rest, seq)
    return jnp.dot(rows, out_weight, preferred_element_type=jnp.float32).astype(jnp.bfloat16)


def solution(mesh):
    placed = (
        P("kv", None), P(), P(None, "tp"), P(None, "tp"), P(None, "tp"), P(None, "tp"), P(None, "tp"), P(),
        P("tp", None, None), P("tp", None, None), P("tp", None, None), P("tp", None, None), P("tp", None, None),
        P("tp", None, None), P(), P("tp", None, None),
    )
    return jax.shard_map(
        per_device, mesh=mesh, in_specs=placed, out_specs=P(("kv", "tp"), None), check_vma=False
    )
```

time: 101 us -> 78.6 us (0.78)
  local copies, waits for them, and re-layouts: 18 us -> 0 us
  Pallas kernels: 79.9 us -> 73.8 us
  matrix products: 2.23 us -> 4.58 us
    unnamed x38 -> x0, local copies, waits for them, and re-layouts: 17.3 us -> none
    pallas_call x2 -> x1, Pallas kernels: 79.9 us -> 73.8 us  [layer(): pl.pallas_call(layer_kernel, in_specs=[pl.BlockSpec(memory_space=pltpu.SM...]
    dot_general x1, matrix products: 2.23 us -> 4.58 us  [per_device(): jnp.dot(rows, out_weight, preferred_element_type=jnp.float32)]
where the time goes in v2:
time: 78.6 us; the launch traced here: 78.4 us
  Pallas kernels  73.8 us (94%)
  matrix products  4.58 us (6%)
    pallas_call x1, Pallas kernels, layer(): pl.pallas_call(layer_kernel, in_specs=[pl.BlockSpec(memory_space=pltpu.SM...  73.8 us
    dot_general x1, matrix products, per_device(): jnp.dot(rows, out_weight, preferred_element_type=jnp.float32)  4.58 us

profile of v2, /device:TPU:1, one launch (start us, length us, event | category | flops | bytes accessed | tf_op | source)
XLA Modules:
  0.0 78.4 jit_solution(819506649894907912)
XLA Ops:
  0.0 73.8 %layer.1 = bf16[256,1024]{1,0:T(8,128)(2,1)} custom-call(s32[1,8,256]{2,1,0:T(8,128)} %bitcast.17, bf16[2048,2048]{1,0:T(8,128)(2,1)} %x_hbm.1, bf16[2048]{0:T(1024)(128)(2,1)} %gain_hbm.1, bf16[2048,128]{1,0:T(8,128)(2,1)} %qw_hbm.1, bf16[64,2048]{1,0:T(8,128)(2,1)} %bitcast.10, bf16[64,2048]{1,0:T(8,128)(2,1)} %bitcast.11, bf16[64,2048]{1,0:T(8,128)(2,1)} %bitcast.12, ...), custom_call_target="tpu_custom_call" | custom-call | tf_op jit(solution)/shard_map/layer/pallas_call | solution.py:342
  73.8 4.6 %convolution_convert_fusion = bf16[256,2048]{1,0:T(8,128)(2,1)} fusion(bf16[256,1024]{1,0:T(8,128)(2,1)} %layer.1, bf16[1024,2048]{1,0:T(8,128)(2,1)} %param.34), kind=kOutput, calls=%fused_computation | convolution fusion | flops 1074266112 | bytes 5767168 | tf_op jit(solution)/shard_map/dot_general | solution.py:382

commit v3 on v2

--- a/solution.py
+++ b/solution.py
@@ -34,44 +34,42 @@
     return 0.5 * x * (1.0 + jnp.tanh(math.sqrt(2.0 / math.pi) * (x + 0.044715 * (x * x * x))))
 
 
-def rel(dz, dx):
-    return (dz % 4) * 4 + dx % 4
-
-
-def transfer_plan():
-    plan = []
-    for q in (0, 2):
-        plan += [("x+", rel(0, 0), q, 2, rel(0, -1)), ("x-", rel(0, 0), q, 2, rel(0, 1))]
-        plan += [("z+", rel(0, 0), q, 2, rel(-1, 0)), ("z-", rel(0, 0), q, 2, rel(1, 0))]
-    plan += [("x+", rel(0, -1), 0, 1, rel(0, 2)), ("x-", rel(0, 1), 1, 1, rel(0, 2))]
-    plan += [("z+", rel(-1, 0), 2, 1, rel(2, 0)), ("z-", rel(1, 0), 3, 1, rel(2, 0))]
-    for d in (-1, 1):
-        plan += [("z+", rel(0, d), 0, 2, rel(-1, d)), ("z-", rel(0, d), 0, 2, rel(1, d))]
-        plan += [("x+", rel(d, 0), 2, 2, rel(d, -1)), ("x-", rel(d, 0), 2, 2, rel(d, 1))]
-    plan += [("z+", rel(-1, 0), 0, 1, rel(2, 0)), ("z-", rel(1, 0), 1, 1, rel(2, 0))]
-    plan += [("x+", rel(0, -1), 2, 1, rel(0, 2)), ("x-", rel(0, 1), 3, 1, rel(0, 2))]
-    plan += [("z+", rel(0, 2), 0, 2, rel(-1, 2)), ("z-", rel(0, 2), 0, 2, rel(1, 2))]
-    plan += [("x+", rel(2, 0), 2, 2, rel(2, -1)), ("x-", rel(2, 0), 2, 2, rel(2, 1))]
-    for d in (-1, 1):
-        plan += [("z+", rel(-1, d), 0, 1, rel(2, d)), ("z-", rel(1, d), 1, 1, rel(2, d))]
-        plan += [("x+", rel(d, -1), 2, 1, rel(d, 2)), ("x-", rel(d, 1), 3, 1, rel(d, 2))]
-    plan += [("z+", rel(-1, 2), 0, 1, rel(2, 2)), ("z-", rel(1, 2), 1, 1, rel(2, 2))]
-    plan += [("x+", rel(2, -1), 2, 1, rel(2, 2)), ("x-", rel(2, 1), 3, 1, rel(2, 2))]
+WAYS = {0: ("x", "z"), 1: ("z", "x")}
+ORDER = (0, 1, 3, 2)
+VIA_PLUS = 24
+
+
+def copy_plan():
+    plan = {}
+    for kind, (first, second) in WAYS.items():
+        plan[kind, "own+"] = (first + "+", "ring", 0, 32, "ring", 96)
+        plan[kind, "own-"] = (first + "-", "ring", 0, 32, "ring", 32)
+        plan[kind, "far+"] = (first + "+", "ring", 96, 16, "ring", 64)
+        plan[kind, "far-"] = (first + "-", "ring", 48, 16, "ring", 80)
+        for name, at, n, half in (("early", 0, 16, 8), ("late", 16, 48, VIA_PLUS)):
+            plan[kind, name + "+"] = (second + "+", "pack", at, n, "slot", 128 + at)
+            plan[kind, name + "-"] = (second + "-", "pack", 128 + at, n, "slot", at)
+            plan[kind, name + "2+"] = (second + "+", "pack", 64 + at, half, "pass", at)
+            plan[kind, name + "2-"] = (second + "-", "pack", 64 + at + half, n - half, "pass", at + half)
+            plan[kind, name + "3+"] = (second + "+", "pass", at, half, "slot", 64 + at)
+            plan[kind, name + "3-"] = (second + "-", "pass", at + half, n - half, "slot", 64 + at + half)
     return plan
 
 
-PLAN = transfer_plan()
+PLAN = copy_plan()
+NAMES = list(PLAN)
 
 
 def layer_kernel(
-    chosen_ref, x_hbm, gain_hbm, qw_hbm, ck_hbm, cv_hbm, sk_hbm, sv_hbm, bw_hbm,
+    chosen_hbm, x_hbm, gain_hbm, qw_hbm, ck_hbm, cv_hbm, sk_hbm, sv_hbm, bw_hbm,
     ke_hbm, ki_hbm, ko_hbm, ve_hbm, vi_hbm, vo_hbm, cl_hbm, sl_hbm, ch_hbm, sh_hbm,
     out_ref,
     x_ref, gain_ref, qw_ref, ck_ref, cv_ref, sk_ref, sv_ref, bw_ref,
     ke_ref, ki_ref, ko_ref, ve_ref, vi_ref, vo_ref, cl_ref, sl_ref, ch_ref, sh_ref,
     w_ref, scale_ref, bi_ref, xk_ref, xv_ref, qp_ref, qt_ref, gate_ref, sum_ref,
-    span_ref, sums_ref, mix_ref, send_ref,
-    in_sem, x_sem, span_send, span_recv, sum_send, sum_recv, tp_send, tp_recv,
+    own_ref, ring_ref, pack_ref, pass_ref, slot_ref, chosen_ref, table_ref, find_ref,
+    sums_ref, mix_ref, send_ref,
+    in_sem, x_sem, find_sem, span_send, span_recv, sum_send, sum_recv, tp_send, tp_recv,
 ):
     me = lax.axis_index("kv")
     tp = lax.axis_index("tp")
@@ -84,14 +82,16 @@
         (cl_hbm, cl_ref), (sl_hbm, sl_ref), (ch_hbm.at[pl.ds(me * 32, 32)], ch_ref),
         (sh_hbm.at[pl.ds(me * 32, 32)], sh_ref), (ke_hbm, ke_ref), (ve_hbm, ve_ref),
         (ki_hbm, ki_ref), (ko_hbm, ko_ref), (vi_hbm, vi_ref), (vo_hbm, vo_ref), (qw_hbm, qw_ref), (bw_hbm, bw_ref),
+        (chosen_hbm, chosen_ref),
     ]
     small = [pltpu.make_async_copy(a, b, in_sem.at[i]) for i, (a, b) in enumerate(small)]
     rows_in = [pltpu.make_async_copy(x_hbm.at[pl.ds(i * ROWS, ROWS)], x_ref.at[i], x_sem.at[i]) for i in range(steps)]
+    small[17].start()
     for copy in small[:9]:
         copy.start()
     for copy in rows_in:
         copy.start()
-    for copy in small[9:]:
+    for copy in small[9:17]:
         copy.start()
 
     barrier = pltpu.get_barrier_semaphore()
@@ -104,6 +104,23 @@
     front = lane < 64
     flip = lane % 64 < 32
     sign = jnp.where(flip, -1.0, 1.0)
+
+    small[17].wait()
+    block = chosen_ref[0]
+    query = lax.broadcasted_iota(jnp.int32, block.shape, 1)
+    for s in range(16):
+        table_ref[s : s + 1, :] = jnp.sum(jnp.where(block // 32 == s, block % 32, 0), axis=0, keepdims=True)
+    usable = block * SEL_BLOCK < query * Q_BLOCK
+    rz = jnp.where(usable, (block // 128 + 4 - mz) % 4, 0)
+    rx = jnp.where(usable, (block // 32 % 4 + 4 - mx) % 4, 0)
+    inside = jnp.where(usable, block % 32, 0)
+    for row, r_first, r_second in ((16, rx, rz), (32, rz, rx)):
+        place = jnp.where(r_first < 2, r_first, 5 - r_first)
+        table_ref[row : row + 8, :] = r_first * 32 + inside
+        table_ref[row + 8 : row + 16, :] = jnp.where(r_second == 0, -1, r_second * 64 - 64 + place * 16 + query % 16)
+    table_ref[48:56, :] = jnp.where(usable, 1, 0)
+    find = pltpu.make_async_copy(table_ref, find_ref, find_sem)
+    find.start()
 
     def angles(step):
         cos, sin = [], []
@@ -140,7 +157,10 @@
         y = lax.dot_general(x, w_ref[...], NT, preferred_element_type=jnp.float32) * scale
         cos, sin = angles(step)
         kv = turn(y[:, 0:128], jnp.where(front, cos, 1.0), jnp.where(front, sin, 0.0)).astype(jnp.bfloat16)
-        span_ref[0, pl.ds(step * (ROWS // 64), ROWS // 64)] = kv.reshape(ROWS // 64, 64, 128)
+        kv = kv.reshape(ROWS // 64, 2, 32, 128)
+        for kind in range(2):
+            own_ref[kind, pl.ds(step * (ROWS // 64), ROWS // 64)] = kv[:, kind]
+            ring_ref[kind, pl.ds(step * (ROWS // 64), ROWS // 64)] = kv[:, kind]
         raw = y[:, 128:256].astype(jnp.bfloat16).astype(jnp.float32)
         bi_ref[pl.ds(pl.multiple_of(step * ROWS, ROWS), ROWS), :] = raw + embed
 
@@ -159,35 +179,45 @@
             device_id=((me + k) % 16, tp), device_id_type=MESH,
         )
 
-    def span_copy(i):
-        way, source, first, n, target = PLAN[i]
+    refs = {"ring": ring_ref, "pack": pack_ref, "pass": pass_ref, "slot": slot_ref}
+
+    def span_copy(*name):
+        way, source, at, n, target, to = PLAN[name]
+        i = NAMES.index(name)
         return pltpu.make_async_remote_copy(
-            src_ref=span_ref.at[source, pl.ds(first * 8, n * 8)],
-            dst_ref=span_ref.at[target, pl.ds(first * 8, n * 8)],
-            send_sem=span_send.at[i], recv_sem=span_recv.at[i],
-            device_id=step_to[way], device_id_type=MESH,
+            src_ref=refs[source].at[name[0], pl.ds(at, n)], dst_ref=refs[target].at[name[0], pl.ds(to, n)],
+            send_sem=span_send.at[i], recv_sem=span_recv.at[i], device_id=step_to[way], device_id_type=MESH,
         )
 
-    brings = {}
-    for i, (_, _, first, n, target) in enumerate(PLAN):
-        for quarter in range(first, first + n):
-            brings[target, quarter] = i
-    arrived = set()
-
-    def start(i):
-        _, source, first, n, _ = PLAN[i]
-        if source:
-            for quarter in range(first, first + n):
-                need = brings[source, quarter]
-                if need not in arrived:
-                    span_copy(need).wait_recv()
-                    arrived.add(need)
-        span_copy(i).start()
-
-    for i in range(4):
-        start(i)
-
-    for copy in small[11:]:
+    def start(*names):
+        for name in names:
+            for kind in range(2):
+                span_copy(kind, name).start()
+
+    def arrive(*names):
+        for name in names:
+            for kind in range(2):
+                span_copy(kind, name).wait_recv()
+
+    def pack(targets, places, source):
+        @pl.loop(0, 16, unroll=2)
+        def _(j):
+            for kind in range(2):
+                for e in targets:
+                    d = e + 1
+                    to = ((mz + d) % 4) * 4 + mx if kind == 0 else mz * 4 + (mx + d) % 4
+                    for place in places:
+                        r = ORDER[place]
+                        span = mz * 4 + (mx + r) % 4 if kind == 0 else ((mz + r) % 4) * 4 + mx
+                        wanted = find_ref[span, to * 16 + j]
+                        pack_ref[kind, e * 64 + place * 16 + j] = source[kind, r * 32 + wanted]
+
+    start("own+", "own-")
+    find.wait()
+    pack((0, 1, 2), (0,), own_ref)
+    start("early+", "early-")
+
+    for copy in small[11:17]:
         copy.wait()
     count = bi_ref.shape[0] // CMP_BLOCK
     for t in range(0, CMP_BLOCK, 2):
@@ -203,8 +233,6 @@
     summary = jnp.concatenate(summary, axis=1).astype(jnp.bfloat16)
     sum_ref[...] = summary
     sums_ref[me] = summary
-    for i in range(4, 8):
-        start(i)
 
     w_ref[0:128, :] = (qw_ref[...].astype(jnp.float32).T * gain).astype(jnp.bfloat16)
     r = lax.broadcasted_iota(jnp.int32, (128, 32), 0)
@@ -216,6 +244,9 @@
     for k in range(1, 16):
         sum_copy(k).start()
 
+    arrive("own+", "own-")
+    start("far+", "far-", "early2+", "early2-")
+
     def by_head(v):
         v = v * (HEAD_DIM**-0.5)
         first = jnp.where(front, v, 0.0)
@@ -231,8 +262,15 @@
         qt_ref[:, at, :] = by_head(turn(q, *angles(step)))
         gate_ref[at, :] = 1.0 / (1.0 + jnp.exp(-y[:, 128:256]))
 
-    for i in range(8, 20):
-        start(i)
+    arrive("far+", "far-")
+    pack((1,), (1, 2, 3), ring_ref)
+    start("late2+", "late2-")
+    arrive("early2+", "early2-")
+    start("early3+", "early3-")
+    pack((0,), (1, 2, 3), ring_ref)
+    start("late+")
+    pack((2,), (1, 2, 3), ring_ref)
+    start("late-")
     for k in range(1, 16):
         sum_copy(k).wait_recv()
 
@@ -241,8 +279,7 @@
     def join(first, second):
         return jnp.where(front, pltpu.roll(first, 64, 1), second)
 
-    @pl.loop(0, 8)
-    def _(t):
+    def compressed(t):
         at = pl.multiple_of(t * 256, 256)
         rows = base + at + lax.broadcasted_iota(jnp.int32, (256, 1), 0)
         limit = (rows + 1) // CMP_BLOCK
@@ -259,12 +296,11 @@
             out.append(o * (gate_ref[pl.ds(at, 256), h : h + 1] / total))
         mix_ref[pl.ds(at, 256), :] = join(*out)
 
-    for i in range(20, len(PLAN)):
-        start(i)
-
-    for i in range(len(PLAN)):
-        if i not in arrived:
-            span_copy(i).wait_recv()
+    pl.loop(0, 4)(compressed)
+    arrive("late2+", "late2-")
+    start("late3+", "late3-")
+    pl.loop(4, 8)(compressed)
+    arrive("early+", "early-", "early3+", "early3-", "late+", "late-", "late3+", "late3-")
 
     triangle = lax.broadcasted_iota(jnp.int32, (128, 128), 1) <= lax.broadcasted_iota(jnp.int32, (128, 128), 0)
     ty, core = tp // 2, tp % 2
@@ -287,13 +323,16 @@
         for half in range(2):
             j = to * 2 + half
             at = pl.multiple_of(j * 128, 128)
-            parts, bias = [span_ref[0, 2 * j], span_ref[0, 2 * j + 1]], []
+            parts = [own_ref[kind, 2 * j + b] for b in range(2) for kind in range(2)]
+            bias = []
             for c in range(FAR_PICKS):
-                block = chosen_ref[0, c, me * 16 + j]
-                span, inside = block // 32, block % 32
-                slot = ((span // 4 + 4 - mz) % 4) * 4 + (span % 4 + 4 - mx) % 4
-                parts.append(span_ref[slot, inside])
-                bias.append(jnp.where(block * 64 < base + at, 0.0, NEG))
+                for kind in range(2):
+                    near = find_ref[16 + 16 * kind + c, me * 16 + j]
+                    far = find_ref[24 + 16 * kind + c, me * 16 + j]
+                    parts.append(
+                        jnp.where(far < 0, ring_ref[kind, near], slot_ref[kind, jnp.maximum(far, 0)])
+                    )
+                bias.append(jnp.where(find_ref[48 + c, me * 16 + j] > 0, 0.0, NEG))
             keys = jnp.concatenate(parts, axis=0)
             q = jnp.concatenate([qt_ref[0, pl.ds(at, 128), :], qt_ref[1, pl.ds(at, 128), :]], axis=0)
             s = lax.dot_general(q, keys, NT, preferred_element_type=jnp.float32)
@@ -326,8 +365,8 @@
         tp_copy(i, target_of(i)).wait_send()
     for k in range(1, 16):
         sum_copy(k).wait_send()
-    for i in range(len(PLAN)):
-        span_copy(i).wait_send()
+    for name in NAMES:
+        span_copy(*name).wait_send()
 
 
 def layer(chosen, tokens, rest, seq):
@@ -338,10 +377,11 @@
     held = [pltpu.VMEM((rows // ROWS, ROWS, width), bf)]
     held += [pltpu.VMEM(a.shape, a.dtype) for a in args[1:-2]]
     held += [pltpu.VMEM((rows // 64, 128), f32)] * 2
+    entry = (32, 128)
     dma = pltpu.SemaphoreType.DMA
     return pl.pallas_call(
         layer_kernel,
-        in_specs=[pl.BlockSpec(memory_space=pltpu.SMEM)] + [pl.BlockSpec(memory_space=pltpu.HBM)] * len(args),
+        in_specs=[pl.BlockSpec(memory_space=pltpu.HBM)] * (len(args) + 1),
         out_specs=pl.BlockSpec(memory_space=pltpu.VMEM),
         out_shape=jax.ShapeDtypeStruct((rows // 8, 1024), bf),
         scratch_shapes=held + [
@@ -354,11 +394,18 @@
             pltpu.VMEM((2, rows, 128), bf),
             pltpu.VMEM((rows, 128), f32),
             pltpu.VMEM((rows // CMP_BLOCK, 128), bf),
-            pltpu.VMEM((spans, rows // 64, 64, 128), bf),
+            pltpu.VMEM((2, 32, *entry), bf),
+            pltpu.VMEM((2, 128, *entry), bf),
+            pltpu.VMEM((2, 192, *entry), bf),
+            pltpu.VMEM((2, 64, *entry), bf),
+            pltpu.VMEM((2, 192, *entry), bf),
+            pltpu.VMEM(chosen.shape, jnp.int32),
+            pltpu.VMEM((56, chosen.shape[-1]), jnp.int32),
+            pltpu.SMEM((56, chosen.shape[-1]), jnp.int32),
             pltpu.VMEM((spans, rows // CMP_BLOCK, 128), bf),
             pltpu.VMEM((rows, 128), f32),
             pltpu.VMEM((8, rows // 8, 128), bf),
-            dma((17,)), dma((rows // ROWS,)), dma((len(PLAN),)), dma((len(PLAN),)),
+            dma((18,)), dma((rows // ROWS,)), dma, dma((len(PLAN),)), dma((len(PLAN),)),
             dma((15,)), dma((15,)), dma((7,)), dma((7,)),
         ],
         compiler_params=pltpu.CompilerParams(collective_id=0, has_side_effects=True, vmem_limit_bytes=67043328),

time: 78.6 us -> 67.4 us (0.86)
  Pallas kernels: 73.8 us -> 62.7 us
    pallas_call x1, Pallas kernels: 73.8 us -> 62.7 us  [layer(): pl.pallas_call(layer_kernel, in_specs=[pl.BlockSpec(memory_space=pltpu.HB...]
where the time goes in v3:
time: 67.4 us; the launch traced here: 67.3 us
  Pallas kernels  62.7 us (93%)
  matrix products  4.58 us (7%)
    pallas_call x1, Pallas kernels, layer(): pl.pallas_call(layer_kernel, in_specs=[pl.BlockSpec(memory_space=pltpu.HB...  62.7 us
    dot_general x1, matrix products, per_device(): jnp.dot(rows, out_weight, preferred_element_type=jnp.float32)  4.58 us

profile of v3, /device:TPU:1, one launch (start us, length us, event | category | flops | bytes accessed | tf_op | source)
XLA Modules:
  0.0 67.3 jit_solution(12524202584662437182)
XLA Ops:
  0.0 62.7 %layer.1 = bf16[256,1024]{1,0:T(8,128)(2,1)} custom-call(s32[1,8,256]{2,1,0:T(8,128)} %bitcast.17, bf16[2048,2048]{1,0:T(8,128)(2,1)} %x_hbm.1, bf16[2048]{0:T(1024)(128)(2,1)} %gain_hbm.1, bf16[2048,128]{1,0:T(8,128)(2,1)} %qw_hbm.1, bf16[64,2048]{1,0:T(8,128)(2,1)} %bitcast.10, bf16[64,2048]{1,0:T(8,128)(2,1)} %bitcast.11, bf16[64,2048]{1,0:T(8,128)(2,1)} %bitcast.12, ...), custom_call_target="tpu_custom_call" | custom-call | tf_op jit(solution)/shard_map/layer/pallas_call | solution.py:382
  62.7 4.6 %convolution_convert_fusion = bf16[256,2048]{1,0:T(8,128)(2,1)} fusion(bf16[256,1024]{1,0:T(8,128)(2,1)} %layer.1, bf16[1024,2048]{1,0:T(8,128)(2,1)} %param.34), kind=kOutput, calls=%fused_computation | convolution fusion | flops 1074266112 | bytes 5767168 | tf_op jit(solution)/shard_map/dot_general | solution.py:429

commit v4 on v3

--- a/solution.py
+++ b/solution.py
@@ -42,17 +42,18 @@
 def copy_plan():
     plan = {}
     for kind, (first, second) in WAYS.items():
-        plan[kind, "own+"] = (first + "+", "ring", 0, 32, "ring", 96)
-        plan[kind, "own-"] = (first + "-", "ring", 0, 32, "ring", 32)
+        for part in (0, 1):
+            plan[kind, f"own{part}+"] = (first + "+", "ring", 16 * part, 16, "ring", 96 + 16 * part)
+            plan[kind, f"own{part}-"] = (first + "-", "ring", 16 * part, 16, "ring", 32 + 16 * part)
         plan[kind, "far+"] = (first + "+", "ring", 96, 16, "ring", 64)
         plan[kind, "far-"] = (first + "-", "ring", 48, 16, "ring", 80)
         for name, at, n, half in (("early", 0, 16, 8), ("late", 16, 48, VIA_PLUS)):
-            plan[kind, name + "+"] = (second + "+", "pack", at, n, "slot", 128 + at)
-            plan[kind, name + "-"] = (second + "-", "pack", 128 + at, n, "slot", at)
+            plan[kind, name + "+"] = (second + "+", "pack", at, n, "all", 256 + at)
+            plan[kind, name + "-"] = (second + "-", "pack", 128 + at, n, "all", 128 + at)
             plan[kind, name + "2+"] = (second + "+", "pack", 64 + at, half, "pass", at)
             plan[kind, name + "2-"] = (second + "-", "pack", 64 + at + half, n - half, "pass", at + half)
-            plan[kind, name + "3+"] = (second + "+", "pass", at, half, "slot", 64 + at)
-            plan[kind, name + "3-"] = (second + "-", "pass", at + half, n - half, "slot", 64 + at + half)
+            plan[kind, name + "3+"] = (second + "+", "pass", at, half, "all", 192 + at)
+            plan[kind, name + "3-"] = (second + "-", "pass", at + half, n - half, "all", 192 + at + half)
     return plan
 
 
@@ -62,14 +63,14 @@
 
 def layer_kernel(
     chosen_hbm, x_hbm, gain_hbm, qw_hbm, ck_hbm, cv_hbm, sk_hbm, sv_hbm, bw_hbm,
-    ke_hbm, ki_hbm, ko_hbm, ve_hbm, vi_hbm, vo_hbm, cl_hbm, sl_hbm, ch_hbm, sh_hbm,
+    ke_hbm, ki_hbm, ko_hbm, ve_hbm, vi_hbm, vo_hbm, cl_hbm, sl_hbm, ch_hbm, sh_hbm, weight_hbm,
     out_ref,
     x_ref, gain_ref, qw_ref, ck_ref, cv_ref, sk_ref, sv_ref, bw_ref,
     ke_ref, ki_ref, ko_ref, ve_ref, vi_ref, vo_ref, cl_ref, sl_ref, ch_ref, sh_ref,
     w_ref, scale_ref, bi_ref, xk_ref, xv_ref, qp_ref, qt_ref, gate_ref, sum_ref,
-    own_ref, ring_ref, pack_ref, pass_ref, slot_ref, chosen_ref, table_ref, find_ref,
-    sums_ref, mix_ref, send_ref,
-    in_sem, x_sem, find_sem, span_send, span_recv, sum_send, sum_recv, tp_send, tp_recv,
+    own_ref, ring_ref, pack_ref, pass_ref, all_ref, chosen_ref, table_ref, find_ref,
+    sums_ref, mix_ref, send_ref, rows_ref, hop_ref, weight_ref, total_ref,
+    in_sem, x_sem, find_sem, weight_sem, span_send, span_recv, sum_send, sum_recv, tp_send, tp_recv,
 ):
     me = lax.axis_index("kv")
     tp = lax.axis_index("tp")
@@ -94,6 +95,9 @@
     for copy in small[9:17]:
         copy.start()
 
+    weight = pltpu.make_async_copy(weight_hbm, weight_ref, weight_sem)
+    weight.start()
+
     barrier = pltpu.get_barrier_semaphore()
     for k in range(1, 16):
         pl.semaphore_signal(barrier, inc=1, device_id=((me + k) % 16, tp), device_id_type=MESH)
@@ -111,14 +115,12 @@
     for s in range(16):
         table_ref[s : s + 1, :] = jnp.sum(jnp.where(block // 32 == s, block % 32, 0), axis=0, keepdims=True)
     usable = block * SEL_BLOCK < query * Q_BLOCK
-    rz = jnp.where(usable, (block // 128 + 4 - mz) % 4, 0)
-    rx = jnp.where(usable, (block // 32 % 4 + 4 - mx) % 4, 0)
-    inside = jnp.where(usable, block % 32, 0)
-    for row, r_first, r_second in ((16, rx, rz), (32, rz, rx)):
+    rz = (block // 128 + 4 - mz) % 4
+    rx = (block // 32 % 4 + 4 - mx) % 4
+    for row, r_first, r_second in ((16, rx, rz), (24, rz, rx)):
         place = jnp.where(r_first < 2, r_first, 5 - r_first)
-        table_ref[row : row + 8, :] = r_first * 32 + inside
-        table_ref[row + 8 : row + 16, :] = jnp.where(r_second == 0, -1, r_second * 64 - 64 + place * 16 + query % 16)
-    table_ref[48:56, :] = jnp.where(usable, 1, 0)
+        at = jnp.where(r_second == 0, r_first * 32 + block % 32, 64 + r_second * 64 + place * 16 + query % 16)
+        table_ref[row : row + 8, :] = jnp.where(usable, at, -1)
     find = pltpu.make_async_copy(table_ref, find_ref, find_sem)
     find.start()
 
@@ -145,11 +147,11 @@
         copy.wait()
     embed = jnp.concatenate([ke_ref[0], ve_ref[0]], axis=1).astype(jnp.float32)
     embed = jnp.concatenate([embed] * (ROWS // CMP_BLOCK), axis=0)
-    for copy in rows_in:
-        copy.wait()
-
-    @pl.loop(0, steps)
-    def _(step):
+
+    def keys_and_values(step):
+        pltpu.make_async_copy(
+            x_hbm.at[pl.ds(pl.multiple_of(step * ROWS, ROWS), ROWS)], x_ref.at[step], x_sem.at[step]
+        ).wait()
         x = x_ref[step]
         xf = x.astype(jnp.float32)
         scale = lax.rsqrt(jnp.sum(xf * xf, axis=1, keepdims=True) * (1.0 / width) + NORM_EPS)
@@ -164,8 +166,6 @@
         raw = y[:, 128:256].astype(jnp.bfloat16).astype(jnp.float32)
         bi_ref[pl.ds(pl.multiple_of(step * ROWS, ROWS), ROWS), :] = raw + embed
 
-    pl.semaphore_wait(barrier, 22)
-
     step_to = {
         "x+": (mz * 4 + (mx + 1) % 4, tp),
         "x-": (mz * 4 + (mx + 3) % 4, tp),
@@ -179,7 +179,7 @@
             device_id=((me + k) % 16, tp), device_id_type=MESH,
         )
 
-    refs = {"ring": ring_ref, "pack": pack_ref, "pass": pass_ref, "slot": slot_ref}
+    refs = {"ring": ring_ref, "pack": pack_ref, "pass": pass_ref, "all": all_ref}
 
     def span_copy(*name):
         way, source, at, n, target, to = PLAN[name]
@@ -212,7 +212,11 @@
                         wanted = find_ref[span, to * 16 + j]
                         pack_ref[kind, e * 64 + place * 16 + j] = source[kind, r * 32 + wanted]
 
-    start("own+", "own-")
+    pl.loop(0, steps // 2)(keys_and_values)
+    pl.semaphore_wait(barrier, 22)
+    start("own0+", "own0-")
+    pl.loop(steps // 2, steps)(keys_and_values)
+    start("own1+", "own1-")
     find.wait()
     pack((0, 1, 2), (0,), own_ref)
     start("early+", "early-")
@@ -244,7 +248,7 @@
     for k in range(1, 16):
         sum_copy(k).start()
 
-    arrive("own+", "own-")
+    arrive("own0+", "own0-", "own1+", "own1-")
     start("far+", "far-", "early2+", "early2-")
 
     def by_head(v):
@@ -271,6 +275,8 @@
     start("late+")
     pack((2,), (1, 2, 3), ring_ref)
     start("late-")
+    for kind in range(2):
+        all_ref[kind, 0:128] = ring_ref[kind]
     for k in range(1, 16):
         sum_copy(k).wait_recv()
 
@@ -311,10 +317,33 @@
         flip = jnp.where(pair == 3, 1 - i % 2, i % 2)
         return ((ty + dy) % 4) * 2 + (core + flip) % 2
 
+    def lanes_of(t):
+        return pl.ds(pl.multiple_of(t * 128, 128), 128)
+
     def tp_copy(i, to):
         return pltpu.make_async_remote_copy(
-            src_ref=send_ref.at[i], dst_ref=out_ref.at[:, pl.ds(pl.multiple_of(tp * 128, 128), 128)],
+            src_ref=send_ref.at[i], dst_ref=rows_ref.at[:, lanes_of(tp)],
             send_sem=tp_send.at[i], recv_sem=tp_recv.at[i], device_id=(me, to), device_id_type=MESH,
+        )
+
+    def direct_copy(i):
+        return pltpu.make_async_remote_copy(
+            src_ref=send_ref.at[i, pl.ds(0, 128)], dst_ref=rows_ref.at[pl.ds(0, 128), lanes_of(tp)],
+            send_sem=tp_send.at[i], recv_sem=tp_recv.at[i], device_id=(me, target_of(i)), device_id_type=MESH,
+        )
+
+    def hop_copy(i):
+        return pltpu.make_async_remote_copy(
+            src_ref=send_ref.at[i, pl.ds(128, 128)], dst_ref=hop_ref.at[i],
+            send_sem=tp_send.at[7 + i], recv_sem=tp_recv.at[7 + i],
+            device_id=(me, (ty + 3) % 4 * 2 + core), device_id_type=MESH,
+        )
+
+    def relay_copy(i):
+        return pltpu.make_async_remote_copy(
+            src_ref=hop_ref.at[i], dst_ref=rows_ref.at[pl.ds(128, 128), lanes_of((ty + 1) % 4 * 2 + core)],
+            send_sem=tp_send.at[9 + i], recv_sem=tp_recv.at[9 + i],
+            device_id=(me, (ty + 3) % 4 * 2 + (core + i) % 2), device_id_type=MESH,
         )
 
     @pl.loop(0, 8)
@@ -326,13 +355,9 @@
             parts = [own_ref[kind, 2 * j + b] for b in range(2) for kind in range(2)]
             bias = []
             for c in range(FAR_PICKS):
-                for kind in range(2):
-                    near = find_ref[16 + 16 * kind + c, me * 16 + j]
-                    far = find_ref[24 + 16 * kind + c, me * 16 + j]
-                    parts.append(
-                        jnp.where(far < 0, ring_ref[kind, near], slot_ref[kind, jnp.maximum(far, 0)])
-                    )
-                bias.append(jnp.where(find_ref[48 + c, me * 16 + j] > 0, 0.0, NEG))
+                places = [find_ref[16 + 8 * kind + c, me * 16 + j] for kind in range(2)]
+                parts += [all_ref[kind, jnp.maximum(places[kind], 0)] for kind in range(2)]
+                bias.append(jnp.where(places[0] < 0, NEG, 0.0))
             keys = jnp.concatenate(parts, axis=0)
             q = jnp.concatenate([qt_ref[0, pl.ds(at, 128), :], qt_ref[1, pl.ds(at, 128), :]], axis=0)
             s = lax.dot_general(q, keys, NT, preferred_element_type=jnp.float32)
@@ -353,15 +378,48 @@
 
             @pl.when(i == 7)
             def _():
-                out_ref[half * 128 : half * 128 + 128, pl.ds(pl.multiple_of(tp * 128, 128), 128)] = mixed
-
-        @pl.when(i < 7)
+                rows_ref[half * 128 : half * 128 + 128, lanes_of(tp)] = mixed
+
+        for two in range(2):
+
+            @pl.when(i == two)
+            def _():
+                direct_copy(two).start()
+                hop_copy(two).start()
+
+        @pl.when((i > 1) & (i < 7))
         def _():
             tp_copy(i, to).start()
 
-    for i in range(7):
-        tp_copy(i, target_of(i)).wait_recv()
-    for i in range(7):
+        @pl.when(i == 4)
+        def _():
+            for two in range(2):
+                hop_copy(two).wait_recv()
+                relay_copy(two).start()
+
+    weight.wait()
+    for pair, away in ((1, 1), (2, 3), (3, 0), (0, 2)):
+        if pair == 0:
+            for i in range(2):
+                direct_copy(i).wait_recv()
+                relay_copy(i).wait_recv()
+        else:
+            for i in range(2 * pair, min(2 * pair + 2, 7)):
+                tp_copy(i, target_of(i)).wait_recv()
+        at = pl.ds(pl.multiple_of((ty + 4 - away) % 4 * 256, 256), 256)
+        part = jnp.dot(rows_ref[:, at], weight_ref[at, :], preferred_element_type=jnp.float32)
+        if pair == 1:
+            total_ref[...] = part
+        elif pair:
+            total_ref[...] += part
+        else:
+            out_ref[...] = (total_ref[...] + part).astype(out_ref.dtype)
+
+    for i in range(2):
+        direct_copy(i).wait_send()
+        hop_copy(i).wait_send()
+        relay_copy(i).wait_send()
+    for i in range(2, 7):
         tp_copy(i, target_of(i)).wait_send()
     for k in range(1, 16):
         sum_copy(k).wait_send()
@@ -369,7 +427,7 @@
         span_copy(*name).wait_send()
 
 
-def layer(chosen, tokens, rest, seq):
+def layer(chosen, tokens, rest, out_weight, seq):
     rows, width = tokens.shape
     args = (tokens, *rest, *rope_tables(seq))
     bf, f32 = jnp.bfloat16, jnp.float32
@@ -381,9 +439,9 @@
     dma = pltpu.SemaphoreType.DMA
     return pl.pallas_call(
         layer_kernel,
-        in_specs=[pl.BlockSpec(memory_space=pltpu.HBM)] * (len(args) + 1),
+        in_specs=[pl.BlockSpec(memory_space=pltpu.HBM)] * (len(args) + 2),
         out_specs=pl.BlockSpec(memory_space=pltpu.VMEM),
-        out_shape=jax.ShapeDtypeStruct((rows // 8, 1024), bf),
+        out_shape=jax.ShapeDtypeStruct((rows // 8, width), bf),
         scratch_shapes=held + [
             pltpu.VMEM((256, width), bf),
             pltpu.VMEM((rows // ROWS, ROWS, 1), f32),
@@ -398,19 +456,23 @@
             pltpu.VMEM((2, 128, *entry), bf),
             pltpu.VMEM((2, 192, *entry), bf),
             pltpu.VMEM((2, 64, *entry), bf),
-            pltpu.VMEM((2, 192, *entry), bf),
+            pltpu.VMEM((2, 320, *entry), bf),
             pltpu.VMEM(chosen.shape, jnp.int32),
-            pltpu.VMEM((56, chosen.shape[-1]), jnp.int32),
-            pltpu.SMEM((56, chosen.shape[-1]), jnp.int32),
+            pltpu.VMEM((32, chosen.shape[-1]), jnp.int32),
+            pltpu.SMEM((32, chosen.shape[-1]), jnp.int32),
             pltpu.VMEM((spans, rows // CMP_BLOCK, 128), bf),
             pltpu.VMEM((rows, 128), f32),
             pltpu.VMEM((8, rows // 8, 128), bf),
-            dma((18,)), dma((rows // ROWS,)), dma, dma((len(PLAN),)), dma((len(PLAN),)),
-            dma((15,)), dma((15,)), dma((7,)), dma((7,)),
+            pltpu.VMEM((rows // 8, 1024), bf),
+            pltpu.VMEM((2, 128, 128), bf),
+            pltpu.VMEM(out_weight.shape, bf),
+            pltpu.VMEM((rows // 8, width), f32),
+            dma((18,)), dma((rows // ROWS,)), dma, dma, dma((len(PLAN),)), dma((len(PLAN),)),
+            dma((15,)), dma((15,)), dma((11,)), dma((11,)),
         ],
         compiler_params=pltpu.CompilerParams(collective_id=0, has_side_effects=True, vmem_limit_bytes=67043328),
         name="layer",
-    )(chosen, *args)
+    )(chosen, *args, out_weight)
 
 
 def per_device(
@@ -425,8 +487,7 @@
         key_embed, key_inner.transpose(0, 2, 1), key_outer,
         value_embed, value_inner.transpose(0, 2, 1), value_outer,
     )
-    rows = layer(chosen.transpose(0, 2, 1), tokens, rest, seq)
-    return jnp.dot(rows, out_weight, preferred_element_type=jnp.float32).astype(jnp.bfloat16)
+    return layer(chosen.transpose(0, 2, 1), tokens, rest, out_weight, seq)
 
 
 def solution(mesh):

time: 67.4 us -> 63.3 us (0.939)
  matrix products: 4.58 us -> 0 us
  local copies, waits for them, and re-layouts: 0 us -> 2.3 us
  Pallas kernels: 62.7 us -> 60.9 us
    dot_general x1 -> x0, matrix products: 4.58 us -> none  [per_device(): jnp.dot(rows, out_weight, preferred_element_type=jnp.float32)]
    unnamed x0 -> x1, local copies, waits for them, and re-layouts: none -> 2.3 us
    pallas_call x1, Pallas kernels: 62.7 us -> 60.9 us  [layer(): pl.pallas_call(layer_kernel, in_specs=[pl.BlockSpec(memory_space=pltpu.HB...]
where the time goes in v4:
time: 63.3 us; the launch traced here: 63.2 us
  Pallas kernels  60.9 us (96%)
  local copies, waits for them, and re-layouts  2.3 us (4%)
    pallas_call x1, Pallas kernels, layer(): pl.pallas_call(layer_kernel, in_specs=[pl.BlockSpec(memory_space=pltpu.HB...  60.9 us
    unnamed x1, local copies, waits for them, and re-layouts  2.3 us

profile of v4, /device:TPU:1, one launch (start us, length us, event | category | flops | bytes accessed | tf_op | source)
XLA Modules:
  0.0 63.2 jit_solution(18230887103666665379)
XLA Ops:
  0.0 60.9 %layer.1 = bf16[256,2048]{1,0:T(8,128)(2,1)} custom-call(s32[1,8,256]{2,1,0:T(8,128)} %bitcast.15, bf16[2048,2048]{1,0:T(8,128)(2,1)} %x_hbm.1, bf16[2048]{0:T(1024)(128)(2,1)} %gain_hbm.1, bf16[2048,128]{1,0:T(8,128)(2,1)} %qw_hbm.1, bf16[64,2048]{1,0:T(8,128)(2,1)} %bitcast.8, bf16[64,2048]{1,0:T(8,128)(2,1)} %bitcast.9, bf16[64,2048]{1,0:T(8,128)(2,1)} %bitcast.10, ...), custom_call_target="tpu_custom_call" | custom-call | tf_op jit(solution)/shard_map/layer/pallas_call | solution.py:440
  60.9 2.3 %copy.22 = bf16[256,2048]{1,0:T(8,128)(2,1)} copy(bf16[256,2048]{1,0:T(8,128)(2,1)} %layer.1) | data formatting | bytes 2097152

commit v5 on v4

--- a/solution.py
+++ b/solution.py
@@ -245,14 +245,14 @@
     pick = jnp.where((r < 4) & (c == want), 1.0, 0.0).astype(jnp.bfloat16)
     gates = jnp.dot(pick, bw_ref[...].reshape(32, width), preferred_element_type=jnp.float32)
     w_ref[128:256, :] = (gates * gain).astype(jnp.bfloat16)
+
+    arrive("own0+", "own0-", "own1+", "own1-")
+    start("far+", "far-", "early2+", "early2-")
     for k in range(1, 16):
         sum_copy(k).start()
 
-    arrive("own0+", "own0-", "own1+", "own1-")
-    start("far+", "far-", "early2+", "early2-")
-
     def by_head(v):
-        v = v * (HEAD_DIM**-0.5)
+        v = v * (HEAD_DIM**-0.5 * math.log2(math.e))
         first = jnp.where(front, v, 0.0)
         second = jnp.where(front, pltpu.roll(v, 64, 1), 0.0)
         return jnp.stack([first, second]).astype(jnp.bfloat16)
@@ -264,7 +264,11 @@
         q = y[:, 0:128]
         qp_ref[:, at, :] = by_head(q)
         qt_ref[:, at, :] = by_head(turn(q, *angles(step)))
-        gate_ref[at, :] = 1.0 / (1.0 + jnp.exp(-y[:, 128:256]))
+        gates = 1.0 / (1.0 + jnp.exp(-y[:, 128:256]))
+        for branch in range(2):
+            gate_ref[branch, at, :] = jnp.where(
+                front, gates[:, 2 * branch : 2 * branch + 1], gates[:, 2 * branch + 1 : 2 * branch + 2]
+            )
 
     arrive("far+", "far-")
     pack((1,), (1, 2, 3), ring_ref)
@@ -282,8 +286,13 @@
 
     base = me * 2048
 
+    def with_totals(keys):
+        return jnp.where(front, jnp.ones((), jnp.bfloat16), keys)
+
     def join(first, second):
-        return jnp.where(front, pltpu.roll(first, 64, 1), second)
+        value = jnp.where(front, pltpu.roll(first, 64, 1), second)
+        total = jnp.where(front, first, pltpu.roll(second, 64, 1))
+        return value / jnp.maximum(total, 0.5)
 
     def compressed(t):
         at = pl.multiple_of(t * 256, 256)
@@ -295,12 +304,9 @@
         for h in range(2):
             s = lax.dot_general(qp_ref[h, pl.ds(at, 256), :], sums, NT, preferred_element_type=jnp.float32)
             s = jnp.where(column < limit, s, NEG)
-            top = jnp.maximum(jnp.max(s, axis=1, keepdims=True), -1e20)
-            p = jnp.exp(s - top)
-            total = jnp.maximum(jnp.sum(p, axis=1, keepdims=True), 0.5)
-            o = jnp.dot(p.astype(jnp.bfloat16), sums, preferred_element_type=jnp.float32)
-            out.append(o * (gate_ref[pl.ds(at, 256), h : h + 1] / total))
-        mix_ref[pl.ds(at, 256), :] = join(*out)
+            p = jnp.exp2(s - jnp.maximum(jnp.max(s, axis=1, keepdims=True), -1e20)).astype(jnp.bfloat16)
+            out.append(jnp.dot(p, with_totals(sums), preferred_element_type=jnp.float32))
+        mix_ref[pl.ds(at, 256), :] = join(*out) * gate_ref[0, pl.ds(at, 256), :]
 
     pl.loop(0, 4)(compressed)
     arrive("late2+", "late2-")
@@ -349,36 +355,37 @@
     @pl.loop(0, 8)
     def _(i):
         to = target_of(i)
+        at = pl.multiple_of(to * 256, 256)
+        keys, score = [], []
         for half in range(2):
             j = to * 2 + half
-            at = pl.multiple_of(j * 128, 128)
             parts = [own_ref[kind, 2 * j + b] for b in range(2) for kind in range(2)]
             bias = []
             for c in range(FAR_PICKS):
                 places = [find_ref[16 + 8 * kind + c, me * 16 + j] for kind in range(2)]
                 parts += [all_ref[kind, jnp.maximum(places[kind], 0)] for kind in range(2)]
                 bias.append(jnp.where(places[0] < 0, NEG, 0.0))
-            keys = jnp.concatenate(parts, axis=0)
-            q = jnp.concatenate([qt_ref[0, pl.ds(at, 128), :], qt_ref[1, pl.ds(at, 128), :]], axis=0)
-            s = lax.dot_general(q, keys, NT, preferred_element_type=jnp.float32)
+            keys.append(jnp.concatenate(parts, axis=0))
+            q = jnp.concatenate([qt_ref[h, pl.ds(at + half * 128, 128), :] for h in range(2)], axis=0)
+            s = lax.dot_general(q, keys[half], NT, preferred_element_type=jnp.float32)
             mine = jnp.where(jnp.concatenate([triangle, triangle], axis=0), s[:, :128], NEG)
             far = [
                 s[:, 128 + 128 * c : 256 + 128 * c] + jnp.where(front, bias[2 * c], bias[2 * c + 1])
                 for c in range(FAR_PICKS // 2)
             ]
-            s = jnp.concatenate([mine, *far], axis=1)
-            p = jnp.exp(s - jnp.max(s, axis=1, keepdims=True))
-            total = jnp.sum(p, axis=1, keepdims=True)
-            o = jnp.dot(p.astype(jnp.bfloat16), keys, preferred_element_type=jnp.float32)
-            gates = gate_ref[pl.ds(at, 128), :]
-            first = o[:128] * (gates[:, 2:3] / total[:128])
-            second = o[128:] * (gates[:, 3:4] / total[128:])
-            mixed = (mix_ref[pl.ds(at, 128), :] + join(first, second)).astype(jnp.bfloat16)
-            send_ref[i, half * 128 : half * 128 + 128, :] = mixed
-
-            @pl.when(i == 7)
-            def _():
-                rows_ref[half * 128 : half * 128 + 128, lanes_of(tp)] = mixed
+            score.append(jnp.concatenate([mine, *far], axis=1))
+        weights = [jnp.exp2(s - jnp.max(s, axis=1, keepdims=True)).astype(jnp.bfloat16) for s in score]
+        out = [
+            jnp.dot(w, with_totals(k), preferred_element_type=jnp.float32) for w, k in zip(weights, keys)
+        ]
+        mixed = [join(o[:128], o[128:]) for o in out]
+        mixed = jnp.concatenate(mixed, axis=0) * gate_ref[1, pl.ds(at, 256), :] + mix_ref[pl.ds(at, 256), :]
+        mixed = mixed.astype(jnp.bfloat16)
+        send_ref[i] = mixed
+
+        @pl.when(i == 7)
+        def _():
+            rows_ref[:, lanes_of(tp)] = mixed
 
         for two in range(2):
 
@@ -450,7 +457,7 @@
             pltpu.VMEM((rows // CMP_BLOCK, CMP_BLOCK * 64), bf),
             pltpu.VMEM((2, rows, 128), bf),
             pltpu.VMEM((2, rows, 128), bf),
-            pltpu.VMEM((rows, 128), f32),
+            pltpu.VMEM((2, rows, 128), f32),
             pltpu.VMEM((rows // CMP_BLOCK, 128), bf),
             pltpu.VMEM((2, 32, *entry), bf),
             pltpu.VMEM((2, 128, *entry), bf),

time: 63.3 us -> 59.5 us (0.940)
  Pallas kernels: 60.9 us -> 57.1 us
    pallas_call x1, Pallas kernels: 60.9 us -> 57.1 us  [layer(): pl.pallas_call(layer_kernel, in_specs=[pl.BlockSpec(memory_space=pltpu.HB...]
where the time goes in v5:
time: 59.5 us; the launch traced here: 59.4 us
  Pallas kernels  57.1 us (96%)
  local copies, waits for them, and re-layouts  2.3 us (4%)
    pallas_call x1, Pallas kernels, layer(): pl.pallas_call(layer_kernel, in_specs=[pl.BlockSpec(memory_space=pltpu.HB...  57.1 us
    unnamed x1, local copies, waits for them, and re-layouts  2.3 us

profile of v5, /device:TPU:1, one launch (start us, length us, event | category | flops | bytes accessed | tf_op | source)
XLA Modules:
  0.0 59.4 jit_solution(2103235493335454640)
XLA Ops:
  0.0 57.1 %layer.1 = bf16[256,2048]{1,0:T(8,128)(2,1)} custom-call(s32[1,8,256]{2,1,0:T(8,128)} %bitcast.15, bf16[2048,2048]{1,0:T(8,128)(2,1)} %x_hbm.1, bf16[2048]{0:T(1024)(128)(2,1)} %gain_hbm.1, bf16[2048,128]{1,0:T(8,128)(2,1)} %qw_hbm.1, bf16[64,2048]{1,0:T(8,128)(2,1)} %bitcast.8, bf16[64,2048]{1,0:T(8,128)(2,1)} %bitcast.9, bf16[64,2048]{1,0:T(8,128)(2,1)} %bitcast.10, ...), custom_call_target="tpu_custom_call" | custom-call | tf_op jit(solution)/shard_map/layer/pallas_call | solution.py:447
  57.1 2.3 %copy.22 = bf16[256,2048]{1,0:T(8,128)(2,1)} copy(bf16[256,2048]{1,0:T(8,128)(2,1)} %layer.1) | data formatting | bytes 2097152

commit v6 on v5

--- a/solution.py
+++ b/solution.py
@@ -36,7 +36,6 @@
 
 WAYS = {0: ("x", "z"), 1: ("z", "x")}
 ORDER = (0, 1, 3, 2)
-VIA_PLUS = 24
 
 
 def copy_plan():
@@ -47,13 +46,16 @@
             plan[kind, f"own{part}-"] = (first + "-", "ring", 16 * part, 16, "ring", 32 + 16 * part)
         plan[kind, "far+"] = (first + "+", "ring", 96, 16, "ring", 64)
         plan[kind, "far-"] = (first + "-", "ring", 48, 16, "ring", 80)
-        for name, at, n, half in (("early", 0, 16, 8), ("late", 16, 48, VIA_PLUS)):
-            plan[kind, name + "+"] = (second + "+", "pack", at, n, "all", 256 + at)
-            plan[kind, name + "-"] = (second + "-", "pack", 128 + at, n, "all", 128 + at)
-            plan[kind, name + "2+"] = (second + "+", "pack", 64 + at, half, "pass", at)
-            plan[kind, name + "2-"] = (second + "-", "pack", 64 + at + half, n - half, "pass", at + half)
-            plan[kind, name + "3+"] = (second + "+", "pass", at, half, "all", 192 + at)
-            plan[kind, name + "3-"] = (second + "-", "pass", at + half, n - half, "all", 192 + at + half)
+        for batch, to in enumerate(("even", "odd")):
+            out, hop = 96 * batch, 32 * batch
+            for name, at, n in ((f"early{batch}", 0, 8), (f"late{batch}", 8, 24)):
+                half = n // 2
+                plan[kind, name + "+"] = (second + "+", "pack", out + at, n, to, 192 + at)
+                plan[kind, name + "-"] = (second + "-", "pack", out + 64 + at, n, to, 128 + at)
+                plan[kind, name + "2+"] = (second + "+", "pack", out + 32 + at, half, "pass", hop + at)
+                plan[kind, name + "2-"] = (second + "-", "pack", out + 32 + at + half, half, "pass", hop + at + half)
+                plan[kind, name + "3+"] = (second + "+", "pass", hop + at, half, to, 160 + at)
+                plan[kind, name + "3-"] = (second + "-", "pass", hop + at + half, half, to, 160 + at + half)
     return plan
 
 
@@ -68,7 +70,7 @@
     x_ref, gain_ref, qw_ref, ck_ref, cv_ref, sk_ref, sv_ref, bw_ref,
     ke_ref, ki_ref, ko_ref, ve_ref, vi_ref, vo_ref, cl_ref, sl_ref, ch_ref, sh_ref,
     w_ref, scale_ref, bi_ref, xk_ref, xv_ref, qp_ref, qt_ref, gate_ref, sum_ref,
-    own_ref, ring_ref, pack_ref, pass_ref, all_ref, chosen_ref, table_ref, find_ref,
+    own_ref, ring_ref, pack_ref, pass_ref, even_ref, odd_ref, chosen_ref, table_ref, find_ref,
     sums_ref, mix_ref, send_ref, rows_ref, hop_ref, weight_ref, total_ref,
     in_sem, x_sem, find_sem, weight_sem, span_send, span_recv, sum_send, sum_recv, tp_send, tp_recv,
 ):
@@ -119,7 +121,7 @@
     rx = (block // 32 % 4 + 4 - mx) % 4
     for row, r_first, r_second in ((16, rx, rz), (24, rz, rx)):
         place = jnp.where(r_first < 2, r_first, 5 - r_first)
-        at = jnp.where(r_second == 0, r_first * 32 + block % 32, 64 + r_second * 64 + place * 16 + query % 16)
+        at = jnp.where(r_second == 0, r_first * 32 + block % 32, 96 + r_second * 32 + place * 8 + query % 16 // 2)
         table_ref[row : row + 8, :] = jnp.where(usable, at, -1)
     find = pltpu.make_async_copy(table_ref, find_ref, find_sem)
     find.start()
@@ -179,7 +181,7 @@
             device_id=((me + k) % 16, tp), device_id_type=MESH,
         )
 
-    refs = {"ring": ring_ref, "pack": pack_ref, "pass": pass_ref, "all": all_ref}
+    refs = {"ring": ring_ref, "pack": pack_ref, "pass": pass_ref, "even": even_ref, "odd": odd_ref}
 
     def span_copy(*name):
         way, source, at, n, target, to = PLAN[name]
@@ -199,8 +201,8 @@
             for kind in range(2):
                 span_copy(kind, name).wait_recv()
 
-    def pack(targets, places, source):
-        @pl.loop(0, 16, unroll=2)
+    def pack(batch, targets, places, source):
+        @pl.loop(0, 8, unroll=2)
         def _(j):
             for kind in range(2):
                 for e in targets:
@@ -209,8 +211,8 @@
                     for place in places:
                         r = ORDER[place]
                         span = mz * 4 + (mx + r) % 4 if kind == 0 else ((mz + r) % 4) * 4 + mx
-                        wanted = find_ref[span, to * 16 + j]
-                        pack_ref[kind, e * 64 + place * 16 + j] = source[kind, r * 32 + wanted]
+                        wanted = find_ref[span, to * 16 + 2 * j + batch]
+                        pack_ref[kind, 96 * batch + e * 32 + place * 8 + j] = source[kind, r * 32 + wanted]
 
     pl.loop(0, steps // 2)(keys_and_values)
     pl.semaphore_wait(barrier, 22)
@@ -218,8 +220,9 @@
     pl.loop(steps // 2, steps)(keys_and_values)
     start("own1+", "own1-")
     find.wait()
-    pack((0, 1, 2), (0,), own_ref)
-    start("early+", "early-")
+    for batch in range(2):
+        pack(batch, (0, 1, 2), (0,), own_ref)
+        start(f"early{batch}+", f"early{batch}-")
 
     for copy in small[11:17]:
         copy.wait()
@@ -247,7 +250,7 @@
     w_ref[128:256, :] = (gates * gain).astype(jnp.bfloat16)
 
     arrive("own0+", "own0-", "own1+", "own1-")
-    start("far+", "far-", "early2+", "early2-")
+    start("far+", "far-", "early02+", "early02-", "early12+", "early12-")
     for k in range(1, 16):
         sum_copy(k).start()
 
@@ -270,17 +273,20 @@
                 front, gates[:, 2 * branch : 2 * branch + 1], gates[:, 2 * branch + 1 : 2 * branch + 2]
             )
 
+    rest = (1, 2, 3)
     arrive("far+", "far-")
-    pack((1,), (1, 2, 3), ring_ref)
-    start("late2+", "late2-")
-    arrive("early2+", "early2-")
-    start("early3+", "early3-")
-    pack((0,), (1, 2, 3), ring_ref)
-    start("late+")
-    pack((2,), (1, 2, 3), ring_ref)
-    start("late-")
+    pack(0, (1,), rest, ring_ref)
+    start("late02+", "late02-")
+    arrive("early02+", "early02-", "early12+", "early12-")
+    start("early03+", "early03-", "early13+", "early13-")
+    pack(0, (0,), rest, ring_ref)
+    start("late0+")
+    pack(0, (2,), rest, ring_ref)
+    start("late0-")
+    pack(1, (0, 1, 2), rest, ring_ref)
     for kind in range(2):
-        all_ref[kind, 0:128] = ring_ref[kind]
+        even_ref[kind, 0:128] = ring_ref[kind]
+        odd_ref[kind, 0:128] = ring_ref[kind]
     for k in range(1, 16):
         sum_copy(k).wait_recv()
 
@@ -309,10 +315,11 @@
         mix_ref[pl.ds(at, 256), :] = join(*out) * gate_ref[0, pl.ds(at, 256), :]
 
     pl.loop(0, 4)(compressed)
-    arrive("late2+", "late2-")
-    start("late3+", "late3-")
+    arrive("late02+", "late02-")
+    start("late03+", "late03-", "late12+", "late12-", "late1+", "late1-")
     pl.loop(4, 8)(compressed)
-    arrive("early+", "early-", "early3+", "early3-", "late+", "late-", "late3+", "late3-")
+    arrive("late12+", "late12-")
+    start("late13+", "late13-")
 
     triangle = lax.broadcasted_iota(jnp.int32, (128, 128), 1) <= lax.broadcasted_iota(jnp.int32, (128, 128), 0)
     ty, core = tp // 2, tp % 2
@@ -326,108 +333,118 @@
     def lanes_of(t):
         return pl.ds(pl.multiple_of(t * 128, 128), 128)
 
-    def tp_copy(i, to):
+    def tp_copy(batch, i, to):
         return pltpu.make_async_remote_copy(
-            src_ref=send_ref.at[i], dst_ref=rows_ref.at[:, lanes_of(tp)],
-            send_sem=tp_send.at[i], recv_sem=tp_recv.at[i], device_id=(me, to), device_id_type=MESH,
+            src_ref=send_ref.at[batch, i], dst_ref=rows_ref.at[pl.ds(batch * 128, 128), lanes_of(tp)],
+            send_sem=tp_send.at[batch * 8 + i], recv_sem=tp_recv.at[batch * 8 + i],
+            device_id=(me, to), device_id_type=MESH,
         )
 
-    def direct_copy(i):
+    def hop_copy(batch):
         return pltpu.make_async_remote_copy(
-            src_ref=send_ref.at[i, pl.ds(0, 128)], dst_ref=rows_ref.at[pl.ds(0, 128), lanes_of(tp)],
-            send_sem=tp_send.at[i], recv_sem=tp_recv.at[i], device_id=(me, target_of(i)), device_id_type=MESH,
-        )
-
-    def hop_copy(i):
-        return pltpu.make_async_remote_copy(
-            src_ref=send_ref.at[i, pl.ds(128, 128)], dst_ref=hop_ref.at[i],
-            send_sem=tp_send.at[7 + i], recv_sem=tp_recv.at[7 + i],
+            src_ref=send_ref.at[batch, 1], dst_ref=hop_ref.at[batch],
+            send_sem=tp_send.at[batch * 8 + 1], recv_sem=tp_recv.at[batch * 8 + 1],
             device_id=(me, (ty + 3) % 4 * 2 + core), device_id_type=MESH,
         )
 
-    def relay_copy(i):
+    def relay_copy(batch):
         return pltpu.make_async_remote_copy(
-            src_ref=hop_ref.at[i], dst_ref=rows_ref.at[pl.ds(128, 128), lanes_of((ty + 1) % 4 * 2 + core)],
-            send_sem=tp_send.at[9 + i], recv_sem=tp_recv.at[9 + i],
-            device_id=(me, (ty + 3) % 4 * 2 + (core + i) % 2), device_id_type=MESH,
+            src_ref=hop_ref.at[batch],
+            dst_ref=rows_ref.at[pl.ds(batch * 128, 128), lanes_of((ty + 1) % 4 * 2 + core)],
+            send_sem=tp_send.at[batch * 8 + 7], recv_sem=tp_recv.at[batch * 8 + 7],
+            device_id=(me, (ty + 3) % 4 * 2 + 1 - core), device_id_type=MESH,
         )
 
-    @pl.loop(0, 8)
-    def _(i):
-        to = target_of(i)
-        at = pl.multiple_of(to * 256, 256)
-        keys, score = [], []
-        for half in range(2):
-            j = to * 2 + half
-            parts = [own_ref[kind, 2 * j + b] for b in range(2) for kind in range(2)]
-            bias = []
-            for c in range(FAR_PICKS):
-                places = [find_ref[16 + 8 * kind + c, me * 16 + j] for kind in range(2)]
-                parts += [all_ref[kind, jnp.maximum(places[kind], 0)] for kind in range(2)]
-                bias.append(jnp.where(places[0] < 0, NEG, 0.0))
-            keys.append(jnp.concatenate(parts, axis=0))
-            q = jnp.concatenate([qt_ref[h, pl.ds(at + half * 128, 128), :] for h in range(2)], axis=0)
-            s = lax.dot_general(q, keys[half], NT, preferred_element_type=jnp.float32)
-            mine = jnp.where(jnp.concatenate([triangle, triangle], axis=0), s[:, :128], NEG)
-            far = [
-                s[:, 128 + 128 * c : 256 + 128 * c] + jnp.where(front, bias[2 * c], bias[2 * c + 1])
-                for c in range(FAR_PICKS // 2)
+    def chosen_branch(batch, all_ref):
+        @pl.loop(0, 4)
+        def _(pair):
+            keys, score, at = [], [], []
+            for half in range(2):
+                j = target_of(2 * pair + half) * 2 + batch
+                at.append(pl.ds(pl.multiple_of(j * 128, 128), 128))
+                parts = [own_ref[kind, 2 * j + b] for b in range(2) for kind in range(2)]
+                bias = []
+                for c in range(FAR_PICKS):
+                    places = [find_ref[16 + 8 * kind + c, me * 16 + j] for kind in range(2)]
+                    parts += [all_ref[kind, jnp.maximum(places[kind], 0)] for kind in range(2)]
+                    bias.append(jnp.where(places[0] < 0, NEG, 0.0))
+                keys.append(jnp.concatenate(parts, axis=0))
+                q = jnp.concatenate([qt_ref[h, at[half], :] for h in range(2)], axis=0)
+                s = lax.dot_general(q, keys[half], NT, preferred_element_type=jnp.float32)
+                mine = jnp.where(jnp.concatenate([triangle, triangle], axis=0), s[:, :128], NEG)
+                far = [
+                    s[:, 128 + 128 * c : 256 + 128 * c] + jnp.where(front, bias[2 * c], bias[2 * c + 1])
+                    for c in range(FAR_PICKS // 2)
+                ]
+                score.append(jnp.concatenate([mine, *far], axis=1))
+            weights = [jnp.exp2(s - jnp.max(s, axis=1, keepdims=True)).astype(jnp.bfloat16) for s in score]
+            out = [
+                jnp.dot(w, with_totals(k), preferred_element_type=jnp.float32) for w, k in zip(weights, keys)
             ]
-            score.append(jnp.concatenate([mine, *far], axis=1))
-        weights = [jnp.exp2(s - jnp.max(s, axis=1, keepdims=True)).astype(jnp.bfloat16) for s in score]
-        out = [
-            jnp.dot(w, with_totals(k), preferred_element_type=jnp.float32) for w, k in zip(weights, keys)
-        ]
-        mixed = [join(o[:128], o[128:]) for o in out]
-        mixed = jnp.concatenate(mixed, axis=0) * gate_ref[1, pl.ds(at, 256), :] + mix_ref[pl.ds(at, 256), :]
-        mixed = mixed.astype(jnp.bfloat16)
-        send_ref[i] = mixed
-
-        @pl.when(i == 7)
-        def _():
-            rows_ref[:, lanes_of(tp)] = mixed
-
-        for two in range(2):
-
-            @pl.when(i == two)
+            mixed = [
+                (join(o[:128], o[128:]) * gate_ref[1, rows, :] + mix_ref[rows, :]).astype(jnp.bfloat16)
+                for o, rows in zip(out, at)
+            ]
+            for half in range(2):
+                send_ref[batch, 2 * pair + half] = mixed[half]
+
+            @pl.when(pair == 0)
             def _():
-                direct_copy(two).start()
-                hop_copy(two).start()
-
-        @pl.when((i > 1) & (i < 7))
-        def _():
-            tp_copy(i, to).start()
-
-        @pl.when(i == 4)
-        def _():
-            for two in range(2):
-                hop_copy(two).wait_recv()
-                relay_copy(two).start()
-
-    weight.wait()
-    for pair, away in ((1, 1), (2, 3), (3, 0), (0, 2)):
+                tp_copy(batch, 0, target_of(0)).start()
+                hop_copy(batch).start()
+
+            @pl.when(pair > 0)
+            def _():
+                tp_copy(batch, 2 * pair, target_of(2 * pair)).start()
+
+            @pl.when((pair > 0) & (pair < 3))
+            def _():
+                tp_copy(batch, 2 * pair + 1, target_of(2 * pair + 1)).start()
+
+            @pl.when(pair == 2)
+            def _():
+                hop_copy(batch).wait_recv()
+                relay_copy(batch).start()
+
+            @pl.when(pair == 3)
+            def _():
+                rows_ref[batch * 128 : batch * 128 + 128, lanes_of(tp)] = mixed[1]
+
+    def rows_arrive(batch, pair):
         if pair == 0:
-            for i in range(2):
-                direct_copy(i).wait_recv()
-                relay_copy(i).wait_recv()
+            tp_copy(batch, 0, target_of(0)).wait_recv()
+            relay_copy(batch).wait_recv()
         else:
             for i in range(2 * pair, min(2 * pair + 2, 7)):
-                tp_copy(i, target_of(i)).wait_recv()
+                tp_copy(batch, i, target_of(i)).wait_recv()
+
+    for batch, all_ref in ((0, even_ref), (1, odd_ref)):
+        for part in ("early", "late"):
+            arrive(*(f"{part}{batch}{way}" for way in ("+", "-", "3+", "3-")))
+        chosen_branch(batch, all_ref)
+
+    weight.wait()
+    for pair in range(4):
+        rows_arrive(0, pair)
+    out_ref[0:128, :] = jnp.dot(rows_ref[0:128, :], weight_ref[...], preferred_element_type=jnp.float32).astype(
+        out_ref.dtype
+    )
+    for pair, away in ((3, 0), (1, 1), (2, 3), (0, 2)):
+        rows_arrive(1, pair)
         at = pl.ds(pl.multiple_of((ty + 4 - away) % 4 * 256, 256), 256)
-        part = jnp.dot(rows_ref[:, at], weight_ref[at, :], preferred_element_type=jnp.float32)
-        if pair == 1:
+        part = jnp.dot(rows_ref[128:256, at], weight_ref[at, :], preferred_element_type=jnp.float32)
+        if pair == 3:
             total_ref[...] = part
         elif pair:
             total_ref[...] += part
         else:
-            out_ref[...] = (total_ref[...] + part).astype(out_ref.dtype)
-
-    for i in range(2):
-        direct_copy(i).wait_send()
-        hop_copy(i).wait_send()
-        relay_copy(i).wait_send()
-    for i in range(2, 7):
-        tp_copy(i, target_of(i)).wait_send()
+            out_ref[128:256, :] = (total_ref[...] + part).astype(out_ref.dtype)
+
+    for batch in range(2):
+        for i in (0, 2, 3, 4, 5, 6):
+            tp_copy(batch, i, target_of(i)).wait_send()
+        hop_copy(batch).wait_send()
+        relay_copy(batch).wait_send()
     for k in range(1, 16):
         sum_copy(k).wait_send()
     for name in NAMES:
@@ -463,19 +480,20 @@
             pltpu.VMEM((2, 128, *entry), bf),
             pltpu.VMEM((2, 192, *entry), bf),
             pltpu.VMEM((2, 64, *entry), bf),
-            pltpu.VMEM((2, 320, *entry), bf),
+            pltpu.VMEM((2, 224, *entry), bf),
+            pltpu.VMEM((2, 224, *entry), bf),
             pltpu.VMEM(chosen.shape, jnp.int32),
             pltpu.VMEM((32, chosen.shape[-1]), jnp.int32),
             pltpu.SMEM((32, chosen.shape[-1]), jnp.int32),
             pltpu.VMEM((spans, rows // CMP_BLOCK, 128), bf),
             pltpu.VMEM((rows, 128), f32),
-            pltpu.VMEM((8, rows // 8, 128), bf),
+            pltpu.VMEM((2, 8, 128, 128), bf),
             pltpu.VMEM((rows // 8, 1024), bf),
             pltpu.VMEM((2, 128, 128), bf),
             pltpu.VMEM(out_weight.shape, bf),
-            pltpu.VMEM((rows // 8, width), f32),
+            pltpu.VMEM((rows // 16, width), f32),
             dma((18,)), dma((rows // ROWS,)), dma, dma, dma((len(PLAN),)), dma((len(PLAN),)),
-            dma((15,)), dma((15,)), dma((11,)), dma((11,)),
+            dma((15,)), dma((15,)), dma((16,)), dma((16,)),
         ],
         compiler_params=pltpu.CompilerParams(collective_id=0, has_side_effects=True, vmem_limit_bytes=67043328),
         name="layer",

time: 59.5 us -> 58.5 us (0.983)
  Pallas kernels: 57.1 us -> 56.1 us
    pallas_call x1, Pallas kernels: 57.1 us -> 56.1 us  [layer(): pl.pallas_call(layer_kernel, in_specs=[pl.BlockSpec(memory_space=pltpu.HB...]
where the time goes in v6:
time: 58.5 us; the launch traced here: 58.4 us
  Pallas kernels  56.1 us (96%)
  local copies, waits for them, and re-layouts  2.3 us (4%)
    pallas_call x1, Pallas kernels, layer(): pl.pallas_call(layer_kernel, in_specs=[pl.BlockSpec(memory_space=pltpu.HB...  56.1 us
    unnamed x1, local copies, waits for them, and re-layouts  2.3 us

profile of v6, /device:TPU:1, one launch (start us, length us, event | category | flops | bytes accessed | tf_op | source)
XLA Modules:
  0.0 58.4 jit_solution(2208205571709594747)
XLA Ops:
  0.0 56.1 %layer.1 = bf16[256,2048]{1,0:T(8,128)(2,1)} custom-call(s32[1,8,256]{2,1,0:T(8,128)} %bitcast.15, bf16[2048,2048]{1,0:T(8,128)(2,1)} %x_hbm.1, bf16[2048]{0:T(1024)(128)(2,1)} %gain_hbm.1, bf16[2048,128]{1,0:T(8,128)(2,1)} %qw_hbm.1, bf16[64,2048]{1,0:T(8,128)(2,1)} %bitcast.8, bf16[64,2048]{1,0:T(8,128)(2,1)} %bitcast.9, bf16[64,2048]{1,0:T(8,128)(2,1)} %bitcast.10, ...), custom_call_target="tpu_custom_call" | custom-call | tf_op jit(solution)/shard_map/layer/pallas_call | solution.py:464
  56.1 2.3 %copy.22 = bf16[256,2048]{1,0:T(8,128)(2,1)} copy(bf16[256,2048]{1,0:T(8,128)(2,1)} %layer.1) | data formatting | bytes 2097152

commit v7 on v6

--- a/solution.py
+++ b/solution.py
@@ -66,13 +66,13 @@
 def layer_kernel(
     chosen_hbm, x_hbm, gain_hbm, qw_hbm, ck_hbm, cv_hbm, sk_hbm, sv_hbm, bw_hbm,
     ke_hbm, ki_hbm, ko_hbm, ve_hbm, vi_hbm, vo_hbm, cl_hbm, sl_hbm, ch_hbm, sh_hbm, weight_hbm,
-    out_ref,
+    out_hbm,
     x_ref, gain_ref, qw_ref, ck_ref, cv_ref, sk_ref, sv_ref, bw_ref,
     ke_ref, ki_ref, ko_ref, ve_ref, vi_ref, vo_ref, cl_ref, sl_ref, ch_ref, sh_ref,
     w_ref, scale_ref, bi_ref, xk_ref, xv_ref, qp_ref, qt_ref, gate_ref, sum_ref,
     own_ref, ring_ref, pack_ref, pass_ref, even_ref, odd_ref, chosen_ref, table_ref, find_ref,
-    sums_ref, mix_ref, send_ref, rows_ref, hop_ref, weight_ref, total_ref,
-    in_sem, x_sem, find_sem, weight_sem, span_send, span_recv, sum_send, sum_recv, tp_send, tp_recv,
+    sums_ref, mix_ref, send_ref, rows_ref, hop_ref, weight_ref, total_ref, stage_ref,
+    in_sem, x_sem, find_sem, weight_sem, leave_sem, span_send, span_recv, sum_send, sum_recv, tp_send, tp_recv,
 ):
     me = lax.axis_index("kv")
     tp = lax.axis_index("tp")
@@ -314,10 +314,10 @@
             out.append(jnp.dot(p, with_totals(sums), preferred_element_type=jnp.float32))
         mix_ref[pl.ds(at, 256), :] = join(*out) * gate_ref[0, pl.ds(at, 256), :]
 
-    pl.loop(0, 4)(compressed)
+    pl.loop(0, 3)(compressed)
     arrive("late02+", "late02-")
     start("late03+", "late03-", "late12+", "late12-", "late1+", "late1-")
-    pl.loop(4, 8)(compressed)
+    pl.loop(3, 8)(compressed)
     arrive("late12+", "late12-")
     start("late13+", "late13-")
 
@@ -401,7 +401,7 @@
             def _():
                 tp_copy(batch, 2 * pair + 1, target_of(2 * pair + 1)).start()
 
-            @pl.when(pair == 2)
+            @pl.when(pair == 3)
             def _():
                 hop_copy(batch).wait_recv()
                 relay_copy(batch).start()
@@ -426,9 +426,11 @@
     weight.wait()
     for pair in range(4):
         rows_arrive(0, pair)
-    out_ref[0:128, :] = jnp.dot(rows_ref[0:128, :], weight_ref[...], preferred_element_type=jnp.float32).astype(
-        out_ref.dtype
+    stage_ref[0] = jnp.dot(rows_ref[0:128, :], weight_ref[...], preferred_element_type=jnp.float32).astype(
+        stage_ref.dtype
     )
+    leave = [pltpu.make_async_copy(stage_ref.at[i], out_hbm.at[i], leave_sem.at[i]) for i in range(2)]
+    leave[0].start()
     for pair, away in ((3, 0), (1, 1), (2, 3), (0, 2)):
         rows_arrive(1, pair)
         at = pl.ds(pl.multiple_of((ty + 4 - away) % 4 * 256, 256), 256)
@@ -438,7 +440,8 @@
         elif pair:
             total_ref[...] += part
         else:
-            out_ref[128:256, :] = (total_ref[...] + part).astype(out_ref.dtype)
+            stage_ref[1] = (total_ref[...] + part).astype(stage_ref.dtype)
+    leave[1].start()
 
     for batch in range(2):
         for i in (0, 2, 3, 4, 5, 6):
@@ -447,6 +450,8 @@
         relay_copy(batch).wait_send()
     for k in range(1, 16):
         sum_copy(k).wait_send()
+    for copy in leave:
+        copy.wait()
     for name in NAMES:
         span_copy(*name).wait_send()
 
@@ -464,8 +469,8 @@
     return pl.pallas_call(
         layer_kernel,
         in_specs=[pl.BlockSpec(memory_space=pltpu.HBM)] * (len(args) + 2),
-        out_specs=pl.BlockSpec(memory_space=pltpu.VMEM),
-        out_shape=jax.ShapeDtypeStruct((rows // 8, width), bf),
+        out_specs=pl.BlockSpec(memory_space=pltpu.HBM),
+        out_shape=jax.ShapeDtypeStruct((2, rows // 16, width), bf),
         scratch_shapes=held + [
             pltpu.VMEM((256, width), bf),
             pltpu.VMEM((rows // ROWS, ROWS, 1), f32),
@@ -492,12 +497,39 @@
             pltpu.VMEM((2, 128, 128), bf),
             pltpu.VMEM(out_weight.shape, bf),
             pltpu.VMEM((rows // 16, width), f32),
-            dma((18,)), dma((rows // ROWS,)), dma, dma, dma((len(PLAN),)), dma((len(PLAN),)),
+            pltpu.VMEM((2, rows // 16, width), bf),
+            dma((18,)), dma((rows // ROWS,)), dma, dma, dma((2,)), dma((len(PLAN),)), dma((len(PLAN),)),
             dma((15,)), dma((15,)), dma((16,)), dma((16,)),
         ],
         compiler_params=pltpu.CompilerParams(collective_id=0, has_side_effects=True, vmem_limit_bytes=67043328),
         name="layer",
     )(chosen, *args, out_weight)
+
+
+def finish_kernel(in_ref, out_ref, held_ref, in_sem, out_sem):
+    n = held_ref.shape[0]
+    come = [pltpu.make_async_copy(in_ref.at[i], held_ref.at[i], in_sem.at[i]) for i in range(n)]
+    go = [pltpu.make_async_copy(held_ref.at[i], out_ref.at[i], out_sem.at[i]) for i in range(n)]
+    for copy in come:
+        copy.start()
+    for a, b in zip(come, go):
+        a.wait()
+        b.start()
+    for copy in go:
+        copy.wait()
+
+
+def finish(rows):
+    shape = (4, rows.shape[1] // 2, rows.shape[2])
+    hbm = pl.BlockSpec(memory_space=pltpu.HBM)
+    return pl.pallas_call(
+        finish_kernel,
+        in_specs=[hbm],
+        out_specs=hbm,
+        out_shape=jax.ShapeDtypeStruct(shape, rows.dtype),
+        scratch_shapes=[pltpu.VMEM(shape, rows.dtype), pltpu.SemaphoreType.DMA((4,)), pltpu.SemaphoreType.DMA((4,))],
+        name="finish",
+    )(rows.reshape(shape)).reshape(-1, rows.shape[2])
 
 
 def per_device(
@@ -512,7 +544,7 @@
         key_embed, key_inner.transpose(0, 2, 1), key_outer,
         value_embed, value_inner.transpose(0, 2, 1), value_outer,
     )
-    return layer(chosen.transpose(0, 2, 1), tokens, rest, out_weight, seq)
+    return finish(layer(chosen.transpose(0, 2, 1), tokens, rest, out_weight, seq))
 
 
 def solution(mesh):

time: 58.5 us -> 56.7 us (0.969)
  local copies, waits for them, and re-layouts: 2.3 us -> 0 us
    unnamed x1 -> x0, local copies, waits for them, and re-layouts: 2.3 us -> none
    pallas_call x0 -> x1, Pallas kernels: none -> 1.98 us  [finish(): pl.pallas_call(finish_kernel, in_specs=[hbm], out_specs=hbm, out_shape=ja...]
    pallas_call x1, Pallas kernels: 56.1 us -> 54.5 us  [layer(): pl.pallas_call(layer_kernel, in_specs=[pl.BlockSpec(memory_space=pltpu.HB...]
where the time goes in v7:
time: 56.7 us; the launch traced here: 56.5 us
  Pallas kernels  56.5 us (100%)
    pallas_call x1, Pallas kernels, layer(): pl.pallas_call(layer_kernel, in_specs=[pl.BlockSpec(memory_space=pltpu.HB...  54.5 us
    pallas_call x1, Pallas kernels, finish(): pl.pallas_call(finish_kernel, in_specs=[hbm], out_specs=hbm, out_shape=ja...  1.98 us

profile of v7, /device:TPU:1, one launch (start us, length us, event | category | flops | bytes accessed | tf_op | source)
XLA Modules:
  0.0 56.5 jit_solution(8124390993714482197)
XLA Ops:
  0.0 54.5 %layer.1 = bf16[2,128,2048]{2,1,0:T(8,128)(2,1)} custom-call(s32[1,8,256]{2,1,0:T(8,128)} %bitcast.18, bf16[2048,2048]{1,0:T(8,128)(2,1)} %x_hbm.1, bf16[2048]{0:T(1024)(128)(2,1)} %gain_hbm.1, bf16[2048,128]{1,0:T(8,128)(2,1)} %qw_hbm.1, bf16[64,2048]{1,0:T(8,128)(2,1)} %bitcast.11, bf16[64,2048]{1,0:T(8,128)(2,1)} %bitcast.12, bf16[64,2048]{1,0:T(8,128)(2,1)} %bitcast.13, ...), custom_call_target="tpu_custom_call" | custom-call | tf_op jit(solution)/shard_map/layer/pallas_call | solution.py:469
  54.5 2.0 %finish.1 = bf16[4,64,2048]{2,1,0:T(8,128)(2,1)} custom-call(bf16[4,64,2048]{2,1,0:T(8,128)(2,1)} %bitcast.10), custom_call_target="tpu_custom_call" | custom-call | tf_op jit(solution)/shard_map/finish/pallas_call | solution.py:525

commit v8 on v7

--- a/solution.py
+++ b/solution.py
@@ -391,7 +391,7 @@
             @pl.when(pair == 0)
             def _():
                 tp_copy(batch, 0, target_of(0)).start()
-                hop_copy(batch).start()
+                (hop_copy(batch) if batch == 0 else tp_copy(batch, 1, target_of(1))).start()
 
             @pl.when(pair > 0)
             def _():
@@ -403,8 +403,9 @@
 
             @pl.when(pair == 3)
             def _():
-                hop_copy(batch).wait_recv()
-                relay_copy(batch).start()
+                if batch == 0:
+                    hop_copy(batch).wait_recv()
+                    relay_copy(batch).start()
 
             @pl.when(pair == 3)
             def _():
@@ -413,7 +414,7 @@
     def rows_arrive(batch, pair):
         if pair == 0:
             tp_copy(batch, 0, target_of(0)).wait_recv()
-            relay_copy(batch).wait_recv()
+            (relay_copy(batch) if batch == 0 else tp_copy(batch, 1, target_of(1))).wait_recv()
         else:
             for i in range(2 * pair, min(2 * pair + 2, 7)):
                 tp_copy(batch, i, target_of(i)).wait_recv()
@@ -446,8 +447,11 @@
     for batch in range(2):
         for i in (0, 2, 3, 4, 5, 6):
             tp_copy(batch, i, target_of(i)).wait_send()
-        hop_copy(batch).wait_send()
-        relay_copy(batch).wait_send()
+        if batch == 0:
+            hop_copy(batch).wait_send()
+            relay_copy(batch).wait_send()
+        else:
+            tp_copy(batch, 1, target_of(1)).wait_send()
     for k in range(1, 16):
         sum_copy(k).wait_send()
     for copy in leave:

time: 56.7 us -> 55.9 us (0.986)
  Pallas kernels: 56.5 us -> 55.8 us
    pallas_call x1, Pallas kernels: 54.5 us -> 53.8 us  [layer(): pl.pallas_call(layer_kernel, in_specs=[pl.BlockSpec(memory_space=pltpu.HB...]
where the time goes in v8:
time: 55.9 us; the launch traced here: 55.8 us
  Pallas kernels  55.8 us (100%)
    pallas_call x1, Pallas kernels, layer(): pl.pallas_call(layer_kernel, in_specs=[pl.BlockSpec(memory_space=pltpu.HB...  53.8 us
    pallas_call x1, Pallas kernels, finish(): pl.pallas_call(finish_kernel, in_specs=[hbm], out_specs=hbm, out_shape=ja...  1.98 us

profile of v8, /device:TPU:1, one launch (start us, length us, event | category | flops | bytes accessed | tf_op | source)
XLA Modules:
  0.0 55.8 jit_solution(5160066481438898353)
XLA Ops:
  0.0 53.8 %layer.1 = bf16[2,128,2048]{2,1,0:T(8,128)(2,1)} custom-call(s32[1,8,256]{2,1,0:T(8,128)} %bitcast.18, bf16[2048,2048]{1,0:T(8,128)(2,1)} %x_hbm.1, bf16[2048]{0:T(1024)(128)(2,1)} %gain_hbm.1, bf16[2048,128]{1,0:T(8,128)(2,1)} %qw_hbm.1, bf16[64,2048]{1,0:T(8,128)(2,1)} %bitcast.11, bf16[64,2048]{1,0:T(8,128)(2,1)} %bitcast.12, bf16[64,2048]{1,0:T(8,128)(2,1)} %bitcast.13, ...), custom_call_target="tpu_custom_call" | custom-call | tf_op jit(solution)/shard_map/layer/pallas_call | solution.py:473
  53.8 2.0 %finish.1 = bf16[4,64,2048]{2,1,0:T(8,128)(2,1)} custom-call(bf16[4,64,2048]{2,1,0:T(8,128)(2,1)} %bitcast.10), custom_call_target="tpu_custom_call" | custom-call | tf_op jit(solution)/shard_map/finish/pallas_call | solution.py:529
